TPU v7x, 256 devices: a whole 4x4x8 slice. The times are simulated.
256 devices in a mesh: sp: 64 (over z, x, core), tp: 4 (over y).
Axes of the slice: x: 4, y: 4, z: 8, core: 2. Of those that a mesh axis runs over, the one named last changes fastest.
Arguments:
- residual_in: bfloat16 [16384, 2048], P(('sp', 'tp')), may hold values from -0.119628906 to 0.119628906
- queries: bfloat16 [16384, 2048], P('sp', 'tp'), may hold values from -6 to 6
- keys_raw: bfloat16 [16384, 512], P('sp', 'tp'), may hold values from -6 to 6
- values_raw: bfloat16 [16384, 512], P('sp', 'tp'), may hold values from -6 to 6
- query_gain: float32 [128], replicated, may hold values from 0.28 to 7
- key_gain: float32 [128], replicated, may hold values from 0.28 to 7
- out_weight: bfloat16 [2048, 2048], P('tp'), may hold values from -0.125 to 0.125
- norm_gain: float32 [2048], replicated, may hold values from 0.1 to 1.9
- gate_weight: bfloat16 [2048, 5632], P('sp', 'tp'), may hold values from -0.125 to 0.125
- up_weight: bfloat16 [2048, 5632], P('sp', 'tp'), may hold values from -0.125 to 0.125
- down_weight: bfloat16 [5632, 2048], P('tp', 'sp'), may hold values from -0.078125 to 0.078125
Outputs:
- residual_out: bfloat16 [16384, 2048], P(('sp', 'tp'))
All inputs are finite; a program needn't handle non-finite values.
Results may differ from a plain program's by a relative error of at most 0.024.
The roundings to bfloat16 on the way count: a program that leaves them out, or rounds other values in their place, can miss the bound.
Values may be sent and summed in bfloat16 or wider, within the bound.
A program may use at most 128 MiB of HBM per device.

v0:
```python
import jax
import jax.numpy as jnp
from jax import lax
from jax.sharding import PartitionSpec as P

GRID_W = 64


EPS = 1e-06
THETA = 10000.0


def in_one_piece(arrays, axis, dim, along):
    both = jnp.concatenate(arrays, axis=along)
    filled, at, done = (lax.all_gather(both, axis, axis=dim, tiled=True), 0, [])
    for a in arrays:
        done.append(lax.slice_in_dim(filled, at, at + a.shape[along], axis=along))
        at += a.shape[along]
    return tuple(done)


def in_blocks(x, dim, length):
    shape = x.shape
    pieces = x.reshape(*shape[:dim], length, shape[dim] // length, *shape[dim + 1 :])
    return jnp.moveaxis(pieces, dim, 0)


def sent_and_summed(x, axis, dim):
    length = lax.axis_size(axis)
    pieces = lax.all_to_all(in_blocks(x, dim, length), axis, 0, 0, tiled=True)
    return jnp.sum(pieces.astype(jnp.float32), axis=0)


def in_order(pieces, dim):
    shape = list(pieces.shape[1:])
    shape[dim] *= pieces.shape[0]
    return jnp.moveaxis(pieces, 0, dim).reshape(shape)


def copy_for_each(x, axis):
    length = lax.axis_size(axis)
    return lax.all_to_all(jnp.broadcast_to(x[None], (length, *x.shape)), axis, 0, 0, tiled=True)


def gathered_copies(x, axis, dim):
    return in_order(copy_for_each(x, axis), dim)


def turn_half(part, angles):
    quarter = part.shape[-1] // 2
    cosine = jnp.cos(angles)[:, None, :]
    sine = jnp.sin(angles)[:, None, :]
    first = part[..., :quarter]
    second = part[..., quarter:]
    return part * cosine + jnp.concatenate([-second, first], axis=-1) * sine


def prepare_heads(raw, gain, positions, heads):
    count = raw.shape[0]
    head_dim = gain.shape[0]
    half = head_dim // 2
    vec = raw.astype(jnp.float32).reshape(count, heads, head_dim)
    vec = vec * lax.rsqrt(jnp.mean(vec * vec, axis=-1, keepdims=True) + EPS) * gain
    freqs = THETA ** (-jnp.arange(0, half, 2, dtype=jnp.float32) / half)
    row_ang = (positions // GRID_W).astype(jnp.float32)[:, None] * freqs
    col_ang = (positions % GRID_W).astype(jnp.float32)[:, None] * freqs
    row_ang = jnp.concatenate([row_ang, row_ang], axis=-1)
    col_ang = jnp.concatenate([col_ang, col_ang], axis=-1)
    turned = jnp.concatenate(
        [turn_half(vec[..., :half], row_ang), turn_half(vec[..., half:], col_ang)], axis=-1
    )
    return turned.astype(jnp.bfloat16)


def per_device(
    residual_in,
    queries,
    keys_raw,
    values_raw,
    query_gain,
    key_gain,
    out_weight,
    norm_gain,
    gate_weight,
    up_weight,
    down_weight,
):
    tok = queries.shape[0]
    head_dim = query_gain.shape[0]
    local_heads = queries.shape[1] // head_dim
    local_kv = keys_raw.shape[1] // head_dim
    group = local_heads // local_kv
    gate_full, up_full = in_one_piece((gate_weight, up_weight), "sp", 0, 1)
    down_full = lax.all_gather(down_weight, "sp", axis=1, tiled=True)
    positions = lax.axis_index("sp") * tok + jnp.arange(tok, dtype=jnp.int32)
    q_rot = prepare_heads(queries, query_gain, positions, local_heads).reshape(
        tok, local_kv, group, head_dim
    )
    k_rot = prepare_heads(keys_raw, key_gain, positions, local_kv)
    vals = values_raw.reshape(tok, local_kv, head_dim)
    start_state = (
        jnp.full((tok, local_kv, group), -jnp.inf, jnp.float32),
        jnp.zeros((tok, local_kv, group), jnp.float32),
        jnp.zeros((tok, local_kv, group, head_dim), jnp.float32),
    )
    carry = start_state
    k_piece, v_piece = in_one_piece((k_rot, vals), "sp", 0, 1)
    length = k_piece.shape[0]
    shards = length // tok
    per_step = max(1, 2048 // tok)
    factor = max((d for d in range(1, shards + 1) if shards % d == 0 and d <= per_step))
    span = factor * tok
    k_blocks = k_piece.reshape(length // span, span, local_kv, head_dim)
    v_blocks = v_piece.reshape(length // span, span, local_kv, head_dim)

    def step(state, blocks):
        top, total, summed = state
        k_blk, v_blk = blocks
        scores = jnp.einsum(
            "qkgd,skd->qkgs", q_rot, k_blk, preferred_element_type=jnp.float32
        ) * head_dim ** (-0.5)
        new_top = jnp.maximum(top, jnp.max(scores, axis=-1))
        shrink = jnp.exp(top - new_top)
        expo = jnp.exp(scores - new_top[..., None])
        total = total * shrink + jnp.sum(expo, axis=-1)
        summed = summed * shrink[..., None] + jnp.einsum(
            "qkgs,skd->qkgd", expo.astype(jnp.bfloat16), v_blk, preferred_element_type=jnp.float32
        )
        return ((new_top, total, summed), None)

    carry, _ = lax.scan(step, carry, (k_blocks, v_blocks))
    top, total, summed = carry
    attended = (summed / total[..., None]).astype(jnp.bfloat16).reshape(tok, local_heads * head_dim)
    projected = sent_and_summed(
        jnp.dot(attended, out_weight, preferred_element_type=jnp.float32).astype(jnp.bfloat16),
        "tp",
        0,
    )
    mixed = (residual_in.astype(jnp.float32) + projected).astype(jnp.bfloat16)
    mixed_f = mixed.astype(jnp.float32)
    normed = (
        mixed_f * lax.rsqrt(jnp.mean(mixed_f * mixed_f, axis=-1, keepdims=True) + EPS) * norm_gain
    ).astype(jnp.bfloat16)
    whole_rows = gathered_copies(normed, "tp", 0)
    gate = jnp.dot(whole_rows, gate_full, preferred_element_type=jnp.float32)
    up_val = jnp.dot(whole_rows, up_full, preferred_element_type=jnp.float32)
    hidden = (jax.nn.silu(gate) * up_val).astype(jnp.bfloat16)
    terms = jnp.dot(hidden, down_full, preferred_element_type=jnp.float32)
    fed = sent_and_summed(terms.astype(jnp.bfloat16), "tp", 0)
    return (mixed_f + 0.5 * fed).astype(jnp.bfloat16)


def solution(mesh):
    placed = (
        P(("sp", "tp"), None),
        P("sp", "tp"),
        P("sp", "tp"),
        P("sp", "tp"),
        P(),
        P(),
        P("tp", None),
        P(),
        P("sp", "tp"),
        P("sp", "tp"),
        P("tp", "sp"),
    )
    return jax.shard_map(
        per_device, mesh=mesh, in_specs=placed, out_specs=P(("sp", "tp"), None), check_vma=False
    )
```

profile of v0, /device:TPU:1, one launch (start us, length us, event | category | flops | bytes accessed | tf_op | source)
XLA Modules:
  0.0 305.7 jit_solution(2898028937360733061)
XLA Ops:
  15.7 84.3 %all-gather.4.cloned.1.call-done = bf16[16384,2,128]{0,2,1:T(8,128)(2,1)} async-done(((bf16[256,2,128]{0,2,1:T(8,128)(2,1)}), bf16[16384,2,128]{0,2,1:T(8,128)(2,1)}) %all-gather.4.cloned.1.call-update) | async-done | bytes 8388624 | tf_op jit(solution)/shard_map/all_gather | solution.py:15
  100.0 5.9 %fusion.70 = (bf16[16384,1,128]{0,2,1:T(8,128)(2,1)}, bf16[16384,1,128]{0,2,1:T(8,128)(2,1)}) fusion(bf16[16384,2,128]{0,2,1:T(8,128)(2,1)} %all-gather.4.cloned.1.call-done), kind=kLoop, calls=%fused_computation.109 | loop fusion | bytes 16777216 | tf_op jit(solution)/shard_map/slice | solution.py:17
  105.9 6.4 %copy.31 = bf16[16384,1,128]{2,0,1:T(8,128)(2,1)} copy(bf16[16384,1,128]{0,2,1:T(8,128)(2,1)} %get-tuple-element.104) | data formatting | bytes 8388608
  112.2 6.4 %copy.26 = bf16[16384,1,128]{2,0,1:T(8,128)(2,1)} copy(bf16[16384,1,128]{0,2,1:T(8,128)(2,1)} %get-tuple-element.103) | data formatting | bytes 8388608 | tf_op jit(solution)/shard_map/slice | solution.py:17
  118.7 104.7 %while.15 = (s32[]{:T(128)}, f32[256,1,4]{0,2,1:T(4,128)S(1)}, f32[256,1,4]{0,2,1:T(4,128)S(1)}, f32[256,1,4,128]{0,3,2,1:T(8,128)S(1)}, bf16[8,2048,1,128]{3,1,...) while((s32[]{:T(128)}, f32[256,1,4]{0,2,1:T(4,128)S(1)}, ...), condition=%wide.region_5.6_spmd.clone, body=%wide.region_2.5_spmd.clone.sunk | while | flops 1090918400 | bytes 61146240 | solution.py:131
  118.7 5.5 %bitcast_reduce_fusion.2 = (f32[256,4]{0,1:T(4,128)S(1)}, f32[2048,256,4]{1,0,2:T(8,128)}) fusion(bf16[256,1,4,128]{3,0,2,1:T(8,128)(2,1)S(1)} %get-tuple-element.203, bf16[8,2048,1,128]{3,1,2,0:T(8,128)(2,1)} %get-tuple-element.202, s32[]{:T(128)} %get-tuple-element.189), kind=kOutput, calls=%fused_computation.1.clone.1 | convolution fusion | flops 541064192 | bytes 9179648 | tf_op jit(solution)/shard_map/while/body/eval_jaxpr/qkgd,skd->qkgs/dot_general | solution.py:119
  124.2 5.5 %fusion.85 = f32[256,1,4,128]{0,3,2,1:T(8,128)S(1)} fusion(f32[2048,256,4]{1,0,2:T(8,128)} %get-tuple-element.178, f32[256,4]{0,1:T(4,128)S(1)} %bitcast.109, f32[256,1,4,128]{0,3,2,1:T(8,128)S(1)} %get-tuple-element.192, bf16[8,2048,1,128]{3,1,0,2:T(8,128)(2,1)} %get-tuple-element.204, s32[]{:T(128)} %get-tuple-element.189, ...), kind=kOutput, calls=%fused_computation.8.clone.1 | convolution fusion | flops 543555584 | bytes 9970177 | tf_op jit(solution)/shard_map/while/body/eval_jaxpr/qkgs,skd->qkgd/dot_general | solution.py:126
  131.6 5.5 %bitcast_reduce_fusion.2 = (f32[256,4]{0,1:T(4,128)S(1)}, f32[2048,256,4]{1,0,2:T(8,128)}) fusion(bf16[256,1,4,128]{3,0,2,1:T(8,128)(2,1)S(1)} %get-tuple-element.203, bf16[8,2048,1,128]{3,1,2,0:T(8,128)(2,1)} %get-tuple-element.202, s32[]{:T(128)} %get-tuple-element.189), kind=kOutput, calls=%fused_computation.1.clone.1 | convolution fusion | flops 541064192 | bytes 9179648 | tf_op jit(solution)/shard_map/while/body/eval_jaxpr/qkgd,skd->qkgs/dot_general | solution.py:119
  137.1 5.5 %fusion.85 = f32[256,1,4,128]{0,3,2,1:T(8,128)S(1)} fusion(f32[2048,256,4]{1,0,2:T(8,128)} %get-tuple-element.178, f32[256,4]{0,1:T(4,128)S(1)} %bitcast.109, f32[256,1,4,128]{0,3,2,1:T(8,128)S(1)} %get-tuple-element.192, bf16[8,2048,1,128]{3,1,0,2:T(8,128)(2,1)} %get-tuple-element.204, s32[]{:T(128)} %get-tuple-element.189, ...), kind=kOutput, calls=%fused_computation.8.clone.1 | convolution fusion | flops 543555584 | bytes 9970177 | tf_op jit(solution)/shard_map/while/body/eval_jaxpr/qkgs,skd->qkgd/dot_general | solution.py:126
  144.5 5.5 %bitcast_reduce_fusion.2 = (f32[256,4]{0,1:T(4,128)S(1)}, f32[2048,256,4]{1,0,2:T(8,128)}) fusion(bf16[256,1,4,128]{3,0,2,1:T(8,128)(2,1)S(1)} %get-tuple-element.203, bf16[8,2048,1,128]{3,1,2,0:T(8,128)(2,1)} %get-tuple-element.202, s32[]{:T(128)} %get-tuple-element.189), kind=kOutput, calls=%fused_computation.1.clone.1 | convolution fusion | flops 541064192 | bytes 9179648 | tf_op jit(solution)/shard_map/while/body/eval_jaxpr/qkgd,skd->qkgs/dot_general | solution.py:119
  150.0 6.1 %fusion.85 = f32[256,1,4,128]{0,3,2,1:T(8,128)S(1)} fusion(f32[2048,256,4]{1,0,2:T(8,128)} %get-tuple-element.178, f32[256,4]{0,1:T(4,128)S(1)} %bitcast.109, f32[256,1,4,128]{0,3,2,1:T(8,128)S(1)} %get-tuple-element.192, bf16[8,2048,1,128]{3,1,0,2:T(8,128)(2,1)} %get-tuple-element.204, s32[]{:T(128)} %get-tuple-element.189, ...), kind=kOutput, calls=%fused_computation.8.clone.1 | convolution fusion | flops 543555584 | bytes 9970177 | tf_op jit(solution)/shard_map/while/body/eval_jaxpr/qkgs,skd->qkgd/dot_general | solution.py:126
  158.0 5.5 %bitcast_reduce_fusion.2 = (f32[256,4]{0,1:T(4,128)S(1)}, f32[2048,256,4]{1,0,2:T(8,128)}) fusion(bf16[256,1,4,128]{3,0,2,1:T(8,128)(2,1)S(1)} %get-tuple-element.203, bf16[8,2048,1,128]{3,1,2,0:T(8,128)(2,1)} %get-tuple-element.202, s32[]{:T(128)} %get-tuple-element.189), kind=kOutput, calls=%fused_computation.1.clone.1 | convolution fusion | flops 541064192 | bytes 9179648 | tf_op jit(solution)/shard_map/while/body/eval_jaxpr/qkgd,skd->qkgs/dot_general | solution.py:119
  163.6 5.7 %fusion.85 = f32[256,1,4,128]{0,3,2,1:T(8,128)S(1)} fusion(f32[2048,256,4]{1,0,2:T(8,128)} %get-tuple-element.178, f32[256,4]{0,1:T(4,128)S(1)} %bitcast.109, f32[256,1,4,128]{0,3,2,1:T(8,128)S(1)} %get-tuple-element.192, bf16[8,2048,1,128]{3,1,0,2:T(8,128)(2,1)} %get-tuple-element.204, s32[]{:T(128)} %get-tuple-element.189, ...), kind=kOutput, calls=%fused_computation.8.clone.1 | convolution fusion | flops 543555584 | bytes 9970177 | tf_op jit(solution)/shard_map/while/body/eval_jaxpr/qkgs,skd->qkgd/dot_general | solution.py:126
  171.4 5.6 %bitcast_reduce_fusion.2 = (f32[256,4]{0,1:T(4,128)S(1)}, f32[2048,256,4]{1,0,2:T(8,128)}) fusion(bf16[256,1,4,128]{3,0,2,1:T(8,128)(2,1)S(1)} %get-tuple-element.203, bf16[8,2048,1,128]{3,1,2,0:T(8,128)(2,1)} %get-tuple-element.202, s32[]{:T(128)} %get-tuple-element.189), kind=kOutput, calls=%fused_computation.1.clone.1 | convolution fusion | flops 541064192 | bytes 9179648 | tf_op jit(solution)/shard_map/while/body/eval_jaxpr/qkgd,skd->qkgs/dot_general | solution.py:119
  177.0 5.7 %fusion.85 = f32[256,1,4,128]{0,3,2,1:T(8,128)S(1)} fusion(f32[2048,256,4]{1,0,2:T(8,128)} %get-tuple-element.178, f32[256,4]{0,1:T(4,128)S(1)} %bitcast.109, f32[256,1,4,128]{0,3,2,1:T(8,128)S(1)} %get-tuple-element.192, bf16[8,2048,1,128]{3,1,0,2:T(8,128)(2,1)} %get-tuple-element.204, s32[]{:T(128)} %get-tuple-element.189, ...), kind=kOutput, calls=%fused_computation.8.clone.1 | convolution fusion | flops 543555584 | bytes 9970177 | tf_op jit(solution)/shard_map/while/body/eval_jaxpr/qkgs,skd->qkgd/dot_general | solution.py:126
  184.7 5.5 %bitcast_reduce_fusion.2 = (f32[256,4]{0,1:T(4,128)S(1)}, f32[2048,256,4]{1,0,2:T(8,128)}) fusion(bf16[256,1,4,128]{3,0,2,1:T(8,128)(2,1)S(1)} %get-tuple-element.203, bf16[8,2048,1,128]{3,1,2,0:T(8,128)(2,1)} %get-tuple-element.202, s32[]{:T(128)} %get-tuple-element.189), kind=kOutput, calls=%fused_computation.1.clone.1 | convolution fusion | flops 541064192 | bytes 9179648 | tf_op jit(solution)/shard_map/while/body/eval_jaxpr/qkgd,skd->qkgs/dot_general | solution.py:119
  197.6 5.5 %bitcast_reduce_fusion.2 = (f32[256,4]{0,1:T(4,128)S(1)}, f32[2048,256,4]{1,0,2:T(8,128)}) fusion(bf16[256,1,4,128]{3,0,2,1:T(8,128)(2,1)S(1)} %get-tuple-element.203, bf16[8,2048,1,128]{3,1,2,0:T(8,128)(2,1)} %get-tuple-element.202, s32[]{:T(128)} %get-tuple-element.189), kind=kOutput, calls=%fused_computation.1.clone.1 | convolution fusion | flops 541064192 | bytes 9179648 | tf_op jit(solution)/shard_map/while/body/eval_jaxpr/qkgd,skd->qkgs/dot_general | solution.py:119
  210.5 5.5 %bitcast_reduce_fusion.2 = (f32[256,4]{0,1:T(4,128)S(1)}, f32[2048,256,4]{1,0,2:T(8,128)}) fusion(bf16[256,1,4,128]{3,0,2,1:T(8,128)(2,1)S(1)} %get-tuple-element.203, bf16[8,2048,1,128]{3,1,2,0:T(8,128)(2,1)} %get-tuple-element.202, s32[]{:T(128)} %get-tuple-element.189), kind=kOutput, calls=%fused_computation.1.clone.1 | convolution fusion | flops 541064192 | bytes 9179648 | tf_op jit(solution)/shard_map/while/body/eval_jaxpr/qkgd,skd->qkgs/dot_general | solution.py:119
  216.0 5.5 %fusion.85 = f32[256,1,4,128]{0,3,2,1:T(8,128)S(1)} fusion(f32[2048,256,4]{1,0,2:T(8,128)} %get-tuple-element.178, f32[256,4]{0,1:T(4,128)S(1)} %bitcast.109, f32[256,1,4,128]{0,3,2,1:T(8,128)S(1)} %get-tuple-element.192, bf16[8,2048,1,128]{3,1,0,2:T(8,128)(2,1)} %get-tuple-element.204, s32[]{:T(128)} %get-tuple-element.189, ...), kind=kOutput, calls=%fused_computation.8.clone.1 | convolution fusion | flops 543555584 | bytes 9970177 | tf_op jit(solution)/shard_map/while/body/eval_jaxpr/qkgs,skd->qkgd/dot_general | solution.py:126
  224.2 18.8 %all_to_all.15 = bf16[4,64,2048]{2,1,0:T(8,128)(2,1)S(1)} all-to-all(bf16[4,64,2048]{2,1,0:T(8,128)(2,1)S(1)} %bitcast.108), channel_id=1, replica_groups=mesh['sp'=64,'tp'=4] {'tp'}, dimensions={0} | all-to-all | bytes 2097152 | tf_op jit(solution)/shard_map/all_to_all | solution.py:30
  243.6 16.5 %all_to_all.16 = bf16[4,64,2048]{2,1,0:T(8,128)(2,1)S(1)} all-to-all(bf16[4,64,2048]{2,1,0:T(8,128)(2,1)S(1)} %broadcast_in_dim.11), channel_id=1, replica_groups=mesh['sp'=64,'tp'=4] {'tp'}, dimensions={0} | all-to-all | bytes 2097152 | tf_op jit(solution)/shard_map/all_to_all | solution.py:42
  260.1 5.7 %fusion.24 = f32[256,1408]{1,0:T(8,128)} fusion(bf16[256,2048]{1,0:T(8,128)(2,1)S(1)} %bitcast.111, bf16[2048,2816]{1,0:T(8,128)(2,1)} %all-gather.6.cloned.1.call-done), kind=kOutput, calls=%fused_computation.26 | convolution fusion | flops 1476395008 | bytes 8257536 | tf_op jit(solution)/shard_map/dot_general | solution.py:145
  270.5 9.2 %convolution_convert_fusion.1 = bf16[256,2048]{1,0:T(8,128)(2,1)} fusion(bf16[1408,2048]{0,1:T(8,128)(2,1)} %all-gather.8.cloned.1.call-done, bf16[256,2048]{1,0:T(8,128)(2,1)S(1)} %bitcast.112, bf16[2048,2816]{1,0:T(8,128)(2,1)} %all-gather.6.cloned.1.call-done, f32[256,1408]{1,0:T(8,128)} %fusion.24), kind=kOutput, calls=%fused_computation.31 | convolution fusion | flops 2955476992 | bytes 15073280 | tf_op jit(solution)/shard_map/dot_general | solution.py:148
  279.6 18.6 %all_to_all.17 = bf16[4,64,2048]{2,1,0:T(8,128)(2,1)S(1)} all-to-all(bf16[4,64,2048]{2,1,0:T(8,128)(2,1)} %bitcast.113), channel_id=1, replica_groups=mesh['sp'=64,'tp'=4] {'tp'}, dimensions={0} | all-to-all | bytes 2097152 | tf_op jit(solution)/shard_map/all_to_all | solution.py:30
  (98 shorter events, 42.2 us)
Async XLA Ops:
  6.5 216.9 %copy-start = (bf16[512,2048]{1,0:T(8,128)(2,1)S(1)}, bf16[512,2048]{1,0:T(8,128)(2,1)}, u32[]{:S(2)}) copy-start(bf16[512,2048]{1,0:T(8,128)(2,1)} %param.19) | copy-start | bytes 6291460
  6.5 93.5 %all-gather.4.cloned.1.call-start = ((), (), s32[]{:S(2)}) async-start(), calls=%async_computation.3 | async-start | bytes 8519680 | tf_op jit(solution)/shard_map/all_gather | solution.py:15
  10.7 249.4 %all-gather.6.cloned.1.call-start = ((), (), s32[]{:S(2)}) async-start(), calls=%async_computation.4 | async-start | bytes 11714560 | tf_op jit(solution)/shard_map/all_gather | solution.py:15
  12.4 258.1 %all-gather.8.cloned.1.call-start = ((), (), s32[]{:S(2)}) async-start(), calls=%async_computation.5 | async-start | bytes 5857280 | tf_op jit(solution)/shard_map/all_gather | solution.py:94
  124.2 6.0 %copy-start.1 = (f32[2048,256,4]{1,0,2:T(8,128)S(1)}, f32[2048,256,4]{1,0,2:T(8,128)}, u32[]{:S(2)}) copy-start(f32[2048,256,4]{1,0,2:T(8,128)} %get-tuple-element.178) | copy-start | bytes 25165828 | tf_op jit(solution)/shard_map/while
  137.1 5.9 %copy-start.1 = (f32[2048,256,4]{1,0,2:T(8,128)S(1)}, f32[2048,256,4]{1,0,2:T(8,128)}, u32[]{:S(2)}) copy-start(f32[2048,256,4]{1,0,2:T(8,128)} %get-tuple-element.178) | copy-start | bytes 25165828 | tf_op jit(solution)/shard_map/while
  150.0 6.6 %copy-start.1 = (f32[2048,256,4]{1,0,2:T(8,128)S(1)}, f32[2048,256,4]{1,0,2:T(8,128)}, u32[]{:S(2)}) copy-start(f32[2048,256,4]{1,0,2:T(8,128)} %get-tuple-element.178) | copy-start | bytes 25165828 | tf_op jit(solution)/shard_map/while
  163.6 6.4 %copy-start.1 = (f32[2048,256,4]{1,0,2:T(8,128)S(1)}, f32[2048,256,4]{1,0,2:T(8,128)}, u32[]{:S(2)}) copy-start(f32[2048,256,4]{1,0,2:T(8,128)} %get-tuple-element.178) | copy-start | bytes 25165828 | tf_op jit(solution)/shard_map/while
  177.0 6.3 %copy-start.1 = (f32[2048,256,4]{1,0,2:T(8,128)S(1)}, f32[2048,256,4]{1,0,2:T(8,128)}, u32[]{:S(2)}) copy-start(f32[2048,256,4]{1,0,2:T(8,128)} %get-tuple-element.178) | copy-start | bytes 25165828 | tf_op jit(solution)/shard_map/while
  190.2 5.9 %copy-start.1 = (f32[2048,256,4]{1,0,2:T(8,128)S(1)}, f32[2048,256,4]{1,0,2:T(8,128)}, u32[]{:S(2)}) copy-start(f32[2048,256,4]{1,0,2:T(8,128)} %get-tuple-element.178) | copy-start | bytes 25165828 | tf_op jit(solution)/shard_map/while
  203.1 6.0 %copy-start.1 = (f32[2048,256,4]{1,0,2:T(8,128)S(1)}, f32[2048,256,4]{1,0,2:T(8,128)}, u32[]{:S(2)}) copy-start(f32[2048,256,4]{1,0,2:T(8,128)} %get-tuple-element.178) | copy-start | bytes 25165828 | tf_op jit(solution)/shard_map/while
  216.0 6.0 %copy-start.1 = (f32[2048,256,4]{1,0,2:T(8,128)S(1)}, f32[2048,256,4]{1,0,2:T(8,128)}, u32[]{:S(2)}) copy-start(f32[2048,256,4]{1,0,2:T(8,128)} %get-tuple-element.178) | copy-start | bytes 25165828 | tf_op jit(solution)/shard_map/while
  223.4 19.7 %copy-start.2 = (bf16[64,2048]{1,0:T(8,128)(2,1)S(1)}, bf16[64,2048]{1,0:T(8,128)(2,1)}, u32[]{:S(2)}) copy-start(bf16[64,2048]{1,0:T(8,128)(2,1)} %param.13) | copy-start | bytes 786436
  223.4 19.9 %copy-start.3 = (f32[2048]{0:T(1024)S(1)}, f32[2048]{0:T(1024)}, u32[]{:S(2)}) copy-start(f32[2048]{0:T(1024)} %param.20) | copy-start | bytes 24580
Sparse Core Ops, SparseCore 0:
  10.8 89.1 all-gather.3
  102.7 88.1 all-gather.5
  193.7 76.7 all-gather.7
where the time goes:
time: 307 us; the launch traced here: 306 us
  matrix products  105 us (34%)
  waiting for transfers between devices  89.7 us (29%)
  blocking collectives  53.9 us (18%)
  local copies, waits for them, and re-layouts  26.1 us (9%)
  other arithmetic  17.6 us (6%)
  between operations  13.3 us (4%)
    all_gather x2, waiting for transfers between devices, in_one_piece(): filled, at, done = (lax.all_gather(both, axis, axis=dim, tiled=True), 0, [])  84.3 us
    dot_general x8, matrix products, step(): jnp.einsum('qkgs,skd->qkgd', expo.astype(jnp.bfloat16), v_blk, preferred_...  45 us
    dot_general x8, matrix products, step(): jnp.einsum('qkgd,skd->qkgs', q_rot, k_blk, preferred_element_type=jnp.flo...  44.2 us
    all_to_all x2, blocking collectives, sent_and_summed(): pieces = lax.all_to_all(in_blocks(x, dim, length), axis, 0, 0, tiled=True)  37.4 us
    all_to_all x1, blocking collectives, copy_for_each(): lax.all_to_all(jnp.broadcast_to(x[None], (length, *x.shape)), axis, 0, 0,...  16.5 us
    slice x2, local copies, waits for them, and re-layouts, in_one_piece(): done.append(lax.slice_in_dim(filled, at, at + a.shape[along], axis=along))  12.3 us
    reduce_sum x8, other arithmetic, step(): total = total * shrink + jnp.sum(expo, axis=-1)  11 us
    unnamed x11, local copies, waits for them, and re-layouts  9.66 us
  transfers between devices with their start and end apart: 3, of which 2 were waited for; matrix products, arithmetic and copies ran while one was open for 43% of the time, Pallas kernels for 0%

commit v1 on v0

v1 whole, which is shorter than its diff:
```python
import functools
import math

import jax
import jax.numpy as jnp
import numpy as np
from jax import lax
from jax.experimental import pallas as pl
from jax.experimental.pallas import tpu as pltpu
from jax.sharding import PartitionSpec as P

GRID_W = 64
EPS = 1e-06
THETA = 10000.0
MESH = pl.DeviceIdType.MESH
NZ, NX = 8, 4
F32 = jnp.float32
BF16 = jnp.bfloat16


def next_hops(color, dz, dx):
    out = []
    if color == 0:
        if dx == 0:
            if 0 <= dz < 4:
                out.append(("z+", dz + 1, 0))
            if -3 < dz <= 0:
                out.append(("z-", dz - 1, 0))
            out.append(("x+", dz, 1))
            out.append(("x-", dz, -1))
        elif dx == 1 and dz % 2 == 0:
            out.append(("x+", dz, 2))
        elif dx == -1 and dz % 2 == 1:
            out.append(("x-", dz, -2))
    else:
        if dz == 0:
            if dx == 0:
                out.append(("x+", 0, 1))
                out.append(("x-", 0, -1))
            elif dx == 1:
                out.append(("x+", 0, 2))
            out.append(("z+", 1, dx))
            out.append(("z-", -1, dx))
        elif dz > 0:
            if dz < (4 if dx % 2 == 0 else 3):
                out.append(("z+", dz + 1, dx))
        else:
            if -dz < (3 if dx % 2 == 0 else 4):
                out.append(("z-", dz - 1, dx))
    return out


def blocks_of(color):
    seen, todo = [], [(0, 0)]
    while todo:
        at = todo.pop(0)
        seen.append(at)
        todo += [(dz, dx) for _, dz, dx in next_hops(color, *at)]
    assert len(seen) == NZ * NX and len({(dz % NZ, dx % NX) for dz, dx in seen}) == NZ * NX
    return seen


def slot_order():
    both = [(abs(dz) + abs(dx), i, color, dz, dx) for color in (0, 1) for i, (dz, dx) in enumerate(blocks_of(color))]
    return [(color, dz, dx) for _, _, color, dz, dx in sorted(both)]


SLOTS = slot_order()
SLOT_OF = {b: i for i, b in enumerate(SLOTS)}
N_SLOTS = len(SLOTS)
PER = 8


def rope(v, gain, cos, sin, lane):
    v = v * lax.rsqrt(jnp.mean(v * v, axis=-1, keepdims=True) + EPS) * gain
    turned = jnp.where(lane % 64 < 32, -pltpu.roll(v, 96, 1), pltpu.roll(v, 32, 1))
    return (v * cos + turned * sin).astype(BF16)


def attention_kernel(
    q_ref, k_ref, v_ref, qg_ref, kg_ref, freq_ref, out_ref,
    kv, qall, acc, top, far_acc, far_top, cos_ref, sin_ref,
    kv_recv, kv_send, swap_recv, swap_send,
):
    me = lax.axis_index("sp")
    core = me % 2
    chip = me // 2
    x = chip % NX
    z = chip // NX
    at = {
        "z+": (((z + 1) % NZ) * NX + x) * 2 + core,
        "z-": (((z + NZ - 1) % NZ) * NX + x) * 2 + core,
        "x+": (z * NX + (x + 1) % NX) * 2 + core,
        "x-": (z * NX + (x + NX - 1) % NX) * 2 + core,
    }
    partner = chip * 2 + 1 - core
    barrier = pltpu.get_barrier_semaphore()
    for dev in (*at.values(), partner):
        pl.semaphore_signal(barrier, inc=1, device_id={"sp": dev}, device_id_type=MESH)

    tok = q_ref.shape[0]
    scale = math.log2(math.e) / math.sqrt(128)
    lane = lax.broadcasted_iota(jnp.int32, (tok, 128), 1)
    token = lax.broadcasted_iota(jnp.int32, (tok, 128), 0) + me * tok
    place = jnp.where(lane < 64, token // GRID_W, token % GRID_W).astype(F32)
    angle = place * freq_ref[...]
    cos_ref[...] = jnp.cos(angle)
    sin_ref[...] = jnp.sin(angle)
    k_rot = rope(k_ref[...].astype(F32), kg_ref[...], cos_ref[...], sin_ref[...], lane)
    for half in (0, 1):
        kv[half, :, 0:128] = k_rot[half * 128 : (half + 1) * 128]
        kv[half, :, 128:256] = v_ref[half * 128 : (half + 1) * 128, :]
    pl.semaphore_wait(barrier, 5)

    def send_on(slot):
        color, dz, dx = SLOTS[slot]
        for link, dz2, dx2 in next_hops(color, dz, dx):
            to = SLOT_OF[(color, dz2, dx2)]
            pltpu.make_async_remote_copy(
                kv.at[slot], kv.at[to], kv_send, kv_recv.at[to],
                device_id={"sp": at[link]}, device_id_type=MESH,
            ).start()

    def arrived(slot):
        pltpu.make_async_remote_copy(
            kv.at[slot], kv.at[slot], kv_send, kv_recv.at[slot],
            device_id={"sp": partner}, device_id_type=MESH,
        ).wait_recv()

    send_on(0)
    send_on(1)

    heads = q_ref.shape[1] // 128
    rows = heads * tok
    for h in range(heads):
        q_rot = rope(
            q_ref[:, h * 128 : (h + 1) * 128].astype(F32), qg_ref[...], cos_ref[...], sin_ref[...], lane
        )
        qall[rows + h * tok : rows + (h + 1) * tok, :] = q_rot
    swap_q = pltpu.make_async_remote_copy(
        qall.at[pl.ds(rows, rows)], qall.at[pl.ds(0, rows)], swap_send.at[0], swap_recv.at[0],
        device_id={"sp": partner}, device_id_type=MESH,
    )
    swap_q.start()
    acc[...] = jnp.zeros_like(acc)
    top[...] = jnp.full_like(top, -1e30)
    for slot in range(2, PER):
        arrived(slot)
        send_on(slot)
    swap_q.wait_recv()

    swap_acc = pltpu.make_async_remote_copy(
        acc.at[pl.ds(0, rows)], far_acc, swap_send.at[1], swap_recv.at[1],
        device_id={"sp": partner}, device_id_type=MESH,
    )
    swap_top = pltpu.make_async_remote_copy(
        top.at[pl.ds(0, rows)], far_top, swap_send.at[2], swap_recv.at[2],
        device_id={"sp": partner}, device_id_type=MESH,
    )
    ones = jnp.ones((PER * 128, 128), BF16)

    def half_step(half, _):
        for k in range(2 * (N_SLOTS // PER - 1)):

            @pl.when(half == k)
            def _():
                first = PER * (k // 2 + 1) + (k % 2) * (PER // 2)
                for slot in range(first, first + PER // 2):
                    arrived(slot)
                    send_on(slot)

        @pl.when(half == 2 * (N_SLOTS // PER) - 1)
        def _():
            swap_acc.start()
            swap_top.start()

        first = (half // 2) * PER
        keys = kv[pl.ds(first, PER), :, 0:128].reshape(PER * 128, 128)
        vals = kv[pl.ds(first, PER), :, 128:256].reshape(PER * 128, 128)
        wide = jnp.concatenate([vals, ones], axis=1)

        def block(i, _):
            r = pl.ds(pl.multiple_of((half % 2) * rows + i * tok, tok), tok)
            s = lax.dot_general(qall[r, :], keys, (((1,), (1,)), ((), ())), preferred_element_type=F32)
            old = top[r, :]
            new = jnp.maximum(old, jnp.max(s, axis=1, keepdims=True))
            top[r, :] = new
            shrink = jnp.exp2((old - new) * scale)
            w = jnp.exp2(s * scale - new[:, 0:1] * scale).astype(BF16)
            o = jnp.dot(w, wide, preferred_element_type=F32)
            acc[r, 0:128] = acc[r, 0:128] * shrink + o[:, 0:128]
            acc[r, 128:256] = acc[r, 128:256] * shrink + o[:, 128:256]
            return 0

        lax.fori_loop(0, heads, block, 0)
        return 0

    lax.fori_loop(0, 2 * (N_SLOTS // PER), half_step, 0)
    swap_acc.wait_recv()
    swap_top.wait_recv()
    for h in range(heads):
        mine = pl.ds(rows + h * tok, tok)
        far = pl.ds(h * tok, tok)
        t1, t2 = top[mine, :], far_top[far, :]
        t = jnp.maximum(t1, t2)
        a1, a2 = jnp.exp2((t1 - t) * scale), jnp.exp2((t2 - t) * scale)
        num = acc[mine, 0:128] * a1 + far_acc[far, 0:128] * a2
        den = acc[mine, 128:256] * a1 + far_acc[far, 128:256] * a2
        out_ref[:, h * 128 : (h + 1) * 128] = (num / den).astype(BF16)
    sent = kv.at[pl.ds(0, N_SLOTS - 2)]
    pltpu.make_async_remote_copy(
        sent, sent, kv_send, kv_recv.at[0], device_id={"sp": partner}, device_id_type=MESH
    ).wait_send()
    swap_q.wait_send()
    swap_acc.wait_send()
    swap_top.wait_send()


def attention(queries, keys_raw, values_raw, query_gain, key_gain):
    tok, width = queries.shape
    rows = tok * width // 128
    freq = (THETA ** (-np.arange(0, 64, 2, dtype=np.float64) / 64)).astype(np.float32)
    freq = jnp.asarray(np.tile(freq, 4)[None])
    vmem = pl.BlockSpec(memory_space=pltpu.VMEM)
    return pl.pallas_call(
        attention_kernel,
        out_shape=jax.ShapeDtypeStruct((tok, width), BF16),
        in_specs=[vmem] * 6,
        out_specs=vmem,
        scratch_shapes=[
            pltpu.VMEM((N_SLOTS, 128, 256), BF16),
            pltpu.VMEM((2 * rows, 128), BF16),
            pltpu.VMEM((2 * rows, 256), F32),
            pltpu.VMEM((2 * rows, 128), F32),
            pltpu.VMEM((rows, 256), F32),
            pltpu.VMEM((rows, 128), F32),
            pltpu.VMEM((tok, 128), F32),
            pltpu.VMEM((tok, 128), F32),
            pltpu.SemaphoreType.DMA((N_SLOTS,)),
            pltpu.SemaphoreType.DMA,
            pltpu.SemaphoreType.DMA((3,)),
            pltpu.SemaphoreType.DMA((3,)),
        ],
        compiler_params=pltpu.CompilerParams(
            collective_id=0, has_side_effects=True, vmem_limit_bytes=40 * 2**20
        ),
        cost_estimate=pl.CostEstimate(flops=9 * 10**9, bytes_accessed=2**22, transcendentals=2**24),
    )(queries, keys_raw, values_raw, query_gain[None], key_gain[None], freq)


def in_blocks(x, dim, length):
    shape = x.shape
    pieces = x.reshape(*shape[:dim], length, shape[dim] // length, *shape[dim + 1 :])
    return jnp.moveaxis(pieces, dim, 0)


def sent_and_summed(x, axis, dim):
    length = lax.axis_size(axis)
    pieces = lax.all_to_all(in_blocks(x, dim, length), axis, 0, 0, tiled=True)
    return jnp.sum(pieces.astype(jnp.float32), axis=0)


def gathered_copies(x, axis):
    length = lax.axis_size(axis)
    pieces = lax.all_to_all(jnp.broadcast_to(x[None], (length, *x.shape)), axis, 0, 0, tiled=True)
    return pieces.reshape(length * x.shape[0], x.shape[1])


def per_device(
    residual_in,
    queries,
    keys_raw,
    values_raw,
    query_gain,
    key_gain,
    out_weight,
    norm_gain,
    gate_weight,
    up_weight,
    down_weight,
):
    units = gate_weight.shape[1]
    weights = jnp.concatenate([gate_weight, up_weight, down_weight.T], axis=1)
    weights = lax.all_gather(weights, "sp", axis=0, tiled=True)
    attended = attention(queries, keys_raw, values_raw, query_gain, key_gain)
    projected = sent_and_summed(
        jnp.dot(attended, out_weight, preferred_element_type=jnp.float32).astype(jnp.bfloat16),
        "tp",
        0,
    )
    mixed = (residual_in.astype(jnp.float32) + projected).astype(jnp.bfloat16)
    mixed_f = mixed.astype(jnp.float32)
    normed = (
        mixed_f * lax.rsqrt(jnp.mean(mixed_f * mixed_f, axis=-1, keepdims=True) + EPS) * norm_gain
    ).astype(jnp.bfloat16)
    whole_rows = gathered_copies(normed, "tp")
    gate = jnp.dot(whole_rows, weights[:, :units], preferred_element_type=jnp.float32)
    up_val = jnp.dot(whole_rows, weights[:, units : 2 * units], preferred_element_type=jnp.float32)
    hidden = (jax.nn.silu(gate) * up_val).astype(jnp.bfloat16)
    terms = lax.dot_general(
        hidden, weights[:, 2 * units :], (((1,), (1,)), ((), ())), preferred_element_type=jnp.float32
    )
    fed = sent_and_summed(terms.astype(jnp.bfloat16), "tp", 0)
    return (mixed_f + 0.5 * fed).astype(jnp.bfloat16)


def solution(mesh):
    placed = (
        P(("sp", "tp"), None),
        P("sp", "tp"),
        P("sp", "tp"),
        P("sp", "tp"),
        P(),
        P(),
        P("tp", None),
        P(),
        P("sp", "tp"),
        P("sp", "tp"),
        P("tp", "sp"),
    )
    return jax.shard_map(
        per_device, mesh=mesh, in_specs=placed, out_specs=P(("sp", "tp"), None), check_vma=False
    )
```

time: 307 us -> 177 us (0.58)
  waiting for transfers between devices: 89.7 us -> 0.02 us
  matrix products: 105 us -> 15.4 us
  Pallas kernels: 0 us -> 88.5 us
  local copies, waits for them, and re-layouts: 26.1 us -> 4.71 us
  other arithmetic: 17.6 us -> 3.27 us
  blocking collectives: 53.9 us -> 49.6 us
    dot_general x18 -> x2, matrix products: 104 us -> 14.7 us  [the longest x1 9.17 us: per_device(): lax.dot_general(hidden, weights[:, 2 * units:], (((1,), (1,)), ((), ())),...]
    all_gather x3 -> x1, waiting for transfers between devices: 89 us -> 0.01 us  [per_device(): weights = lax.all_gather(weights, 'sp', axis=0, tiled=True)]
    pallas_call x0 -> x1, Pallas kernels: none -> 88.5 us  [attention(): pl.pallas_call(attention_kernel, out_shape=jax.ShapeDtypeStruct((tok, wid...]
    slice x2 -> x0, local copies, waits for them, and re-layouts: 12.3 us -> none  [in_one_piece(): done.append(lax.slice_in_dim(filled, at, at + a.shape[along], axis=along))]
    reduce_sum x10 -> x0, other arithmetic: 11.1 us -> none  [the longest x8 11 us: step(): total = total * shrink + jnp.sum(expo, axis=-1)]
    unnamed x11 -> x18, local copies, waits for them, and re-layouts: 9.66 us -> 4.6 us
    while x24 -> x0, local copies, waits for them, and re-layouts: 4.06 us -> none
    all_to_all x2, blocking collectives: 37.4 us -> 33.8 us  [sent_and_summed(): pieces = lax.all_to_all(in_blocks(x, dim, length), axis, 0, 0, tiled=True)]
  transfers between devices with their start and end apart: 3 -> 1, of which waited for: 2 -> 0; matrix products, arithmetic and copies ran while one was open for 43% -> 1% of each run, Pallas kernels for 0% -> 51%
where the time goes in v1:
time: 177 us; the launch traced here: 175 us
  Pallas kernels  88.5 us (50%)
  blocking collectives  49.6 us (28%)
  matrix products  15.4 us (9%)
  between operations  13.5 us (8%)
  local copies, waits for them, and re-layouts  4.71 us (3%)
  other arithmetic  3.27 us (2%)
    pallas_call x1, Pallas kernels, attention(): pl.pallas_call(attention_kernel, out_shape=jax.ShapeDtypeStruct((tok, wid...  88.5 us
    all_to_all x2, blocking collectives, sent_and_summed(): pieces = lax.all_to_all(in_blocks(x, dim, length), axis, 0, 0, tiled=True)  33.8 us
    all_to_all x1, blocking collectives, gathered_copies(): lax.all_to_all(jnp.broadcast_to(x[None], (length, *x.shape)), axis, 0, 0,...  15.7 us
    dot_general x1, matrix products, per_device(): lax.dot_general(hidden, weights[:, 2 * units:], (((1,), (1,)), ((), ())),...  9.17 us
    dot_general x1, matrix products, per_device(): jnp.dot(whole_rows, weights[:, :units], preferred_element_type=jnp.float32)  5.56 us
    unnamed x18, local copies, waits for them, and re-layouts  4.6 us
  transfers between devices with their start and end apart: 1, of which 0 were waited for; matrix products, arithmetic and copies ran while one was open for 1% of the time, Pallas kernels for 51%

profile of v1, /device:TPU:1, one launch (start us, length us, event | category | flops | bytes accessed | tf_op | source)
XLA Modules:
  0.0 175.0 jit_solution(18118272403721345555)
XLA Ops:
  6.5 1.9 %pad_maximum_fusion = bf16[32,4224]{1,0:T(8,128)(2,1)} fusion(bf16[32,1408]{1,0:T(8,128)(2,1)} %bitcast.16, bf16[32,1408]{1,0:T(8,128)(2,1)} %param.21, bf16[32,1408]{1,0:T(8,128)(2,1)} %param.20), kind=kLoop, calls=%fused_computation.26 | loop fusion | flops 811008 | bytes 540672 | tf_op jit(solution)/shard_map/concatenate | solution.py:283
  8.4 0.0 all-gather.2.cloned.1.call-update
  8.4 0.0 copy-start.1
  8.4 0.9 copy-done.1
  9.4 0.8 copy-done.2
  10.2 0.8 copy-done.3
  11.1 0.7 copy-done.4
  11.7 0.7 copy-done.5
  12.4 0.7 copy-done.6
  13.0 88.5 %shard_map.118 = bf16[256,512]{1,0:T(8,128)(2,1)S(1)} custom-call(bf16[256,512]{1,0:T(8,128)(2,1)S(1)} %copy-done.1, bf16[256,128]{1,0:T(8,128)(2,1)S(1)} %copy-done.2, bf16[256,128]{1,0:T(8,128)(2,1)S(1)} %copy-done.3, f32[1,128]{1,0:T(1,128)S(1)} %bitcast.10, f32[1,128]{1,0:T(1,128)S(1)} %bitcast.11, f32[1,128]{1,0:T(1,128)S(1)} %copy-done.6), custom_call_target="tpu_custom_call" | custom-call | flops 8999999488 | bytes 4194304 | tf_op jit(solution)/shard_map/pallas_call | solution.py:225
  101.5 0.7 convolution_convert_fusion
  102.2 0.0 copy-start.7
  102.2 0.0 copy-start.8
  102.2 18.2 %all_to_all.15 = bf16[4,64,2048]{2,1,0:T(8,128)(2,1)S(1)} all-to-all(bf16[4,64,2048]{2,1,0:T(8,128)(2,1)S(1)} %bitcast.12), channel_id=1, replica_groups=mesh['sp'=64,'tp'=4] {'tp'}, dimensions={0} | all-to-all | bytes 2097152 | tf_op jit(solution)/shard_map/all_to_all | solution.py:259
  120.4 0.2 convert_reduce_fusion.1
  120.6 0.2 fusion.23
  120.8 0.1 fusion.25
  120.9 0.1 broadcast_in_dim.16
  121.1 15.7 %all_to_all.16 = bf16[4,64,2048]{2,1,0:T(8,128)(2,1)S(1)} all-to-all(bf16[4,64,2048]{2,1,0:T(8,128)(2,1)S(1)} %broadcast_in_dim.16), channel_id=1, replica_groups=mesh['sp'=64,'tp'=4] {'tp'}, dimensions={0} | all-to-all | bytes 2097152 | tf_op jit(solution)/shard_map/all_to_all | solution.py:265
  136.8 5.6 %fusion.4 = f32[256,1408]{1,0:T(8,128)} fusion(bf16[256,2048]{1,0:T(8,128)(2,1)S(1)} %bitcast.13, bf16[2048,4224]{1,0:T(8,128)(2,1)} %all-gather.2.cloned.1.call-done), kind=kOutput, calls=%fused_computation.4 | convolution fusion | flops 1476395008 | bytes 8257536 | tf_op jit(solution)/shard_map/dot_general | solution.py:297
  142.4 9.2 %fusion.12 = bf16[256,2048]{1,0:T(8,128)(2,1)} fusion(bf16[2048,4224]{1,0:T(8,128)(2,1)} %all-gather.2.cloned.1.call-done, bf16[256,2048]{1,0:T(8,128)(2,1)S(1)} %bitcast.14, f32[256,1408]{1,0:T(8,128)} %fusion.4), kind=kOutput, calls=%fused_computation.9 | convolution fusion | flops 2955476992 | bytes 15073280 | tf_op jit(solution)/shard_map/dot_general | solution.py:300
  151.5 15.7 %all_to_all.17 = bf16[4,64,2048]{2,1,0:T(8,128)(2,1)S(1)} all-to-all(bf16[4,64,2048]{2,1,0:T(8,128)(2,1)} %bitcast.15), channel_id=1, replica_groups=mesh['sp'=64,'tp'=4] {'tp'}, dimensions={0} | all-to-all | bytes 2097152 | tf_op jit(solution)/shard_map/all_to_all | solution.py:259
  167.2 0.2 convert_reduce_fusion
  167.4 0.8 fusion.26
  (12 shorter events, 0.0 us)
Async XLA Ops:
  6.5 95.0 %copy-start = (bf16[512,2048]{1,0:T(8,128)(2,1)S(1)}, bf16[512,2048]{1,0:T(8,128)(2,1)}, u32[]{:S(2)}) copy-start(bf16[512,2048]{1,0:T(8,128)(2,1)} %param.18) | copy-start | bytes 6291460
  6.5 130.3 %all-gather.2.cloned.1.call-start = ((), (), s32[]{:S(2)}) async-start(), calls=%async_computation.3 | async-start | bytes 17571840 | tf_op jit(solution)/shard_map/all_gather | solution.py:284
  8.4 1.0 copy-start.1
  9.4 0.8 copy-start.2
  10.2 0.8 copy-start.3
  11.1 0.7 copy-start.4
  11.7 0.7 copy-start.5
  12.4 0.7 copy-start.6
  102.2 18.4 %copy-start.7 = (bf16[64,2048]{1,0:T(8,128)(2,1)S(1)}, bf16[64,2048]{1,0:T(8,128)(2,1)}, u32[]{:S(2)}) copy-start(bf16[64,2048]{1,0:T(8,128)(2,1)} %param.12) | copy-start | bytes 786436
  102.2 18.6 %copy-start.8 = (f32[2048]{0:T(1024)S(1)}, f32[2048]{0:T(1024)}, u32[]{:S(2)}) copy-start(f32[2048]{0:T(1024)} %param.19) | copy-start | bytes 24580
Sparse Core Ops, SparseCore 0:
  10.1 107.4 all-gather.1

commit v2 on v1

v2 whole, which is shorter than its diff:
```python
import math

import jax
import jax.numpy as jnp
import numpy as np
from jax import lax
from jax.experimental import pallas as pl
from jax.experimental.pallas import tpu as pltpu
from jax.sharding import PartitionSpec as P

GRID_W = 64
EPS = 1e-06
THETA = 10000.0
MESH = pl.DeviceIdType.MESH
NZ, NX = 8, 4
F32 = jnp.float32
BF16 = jnp.bfloat16


def next_hops(color, dz, dx):
    out = []
    if color == 0:
        if dx == 0:
            if 0 <= dz < 4:
                out.append(("z+", dz + 1, 0))
            if -3 < dz <= 0:
                out.append(("z-", dz - 1, 0))
            out.append(("x+", dz, 1))
            out.append(("x-", dz, -1))
        elif dx == 1 and dz % 2 == 0:
            out.append(("x+", dz, 2))
        elif dx == -1 and dz % 2 == 1:
            out.append(("x-", dz, -2))
    else:
        if dz == 0:
            if dx == 0:
                out.append(("x+", 0, 1))
                out.append(("x-", 0, -1))
            elif dx == 1:
                out.append(("x+", 0, 2))
            out.append(("z+", 1, dx))
            out.append(("z-", -1, dx))
        elif dz > 0:
            if dz < (4 if dx % 2 == 0 else 3):
                out.append(("z+", dz + 1, dx))
        else:
            if -dz < (3 if dx % 2 == 0 else 4):
                out.append(("z-", dz - 1, dx))
    return out


def blocks_of(color):
    seen, todo = [], [(0, 0)]
    while todo:
        at = todo.pop(0)
        seen.append(at)
        todo += [(dz, dx) for _, dz, dx in next_hops(color, *at)]
    assert len(seen) == NZ * NX and len({(dz % NZ, dx % NX) for dz, dx in seen}) == NZ * NX
    return seen


def slot_order():
    both = [(abs(dz) + abs(dx), i, color, dz, dx) for color in (0, 1) for i, (dz, dx) in enumerate(blocks_of(color))]
    return [(color, dz, dx) for _, _, color, dz, dx in sorted(both)]


SLOTS = slot_order()
SLOT_OF = {b: i for i, b in enumerate(SLOTS)}
N_SLOTS = len(SLOTS)
PER = 8
BLOCK = 128


def rope(v, gain, cos, sin, lane):
    v = v * lax.rsqrt(jnp.mean(v * v, axis=-1, keepdims=True) + EPS) * gain
    turned = jnp.where(lane % 64 < 32, -pltpu.roll(v, 96, 1), pltpu.roll(v, 32, 1))
    return (v * cos + turned * sin).astype(BF16)


def half(k):
    return pl.ds(k * 1024, 1024)


def layer_kernel(
    res_in, q_in, k_in, v_in, qg_in, kg_in, wo_in, ng_in, gate_in, up_in, down_in, freq_in, out_ref,
    kv, qall, acc, top, far_acc, far_top, cos_ref, sin_ref,
    res_ref, q_ref, k_ref, qg_ref, kg_ref, wo_ref, ng_ref, freq_ref,
    wbuf, att, terms, sums, parts, rows_ref, hidden,
    in_sem, kv_recv, kv_send, swap_recv, swap_send,
    w_recv, w_send, d2d_recv, d2d_send, rs_recv, rs_send, ag_recv, ag_send,
):
    me = lax.axis_index("sp")
    y = lax.axis_index("tp")
    core = me % 2
    chip = me // 2
    x = chip % NX
    z = chip // NX
    zs = {d: (z + NZ - d) % NZ for d in range(-4, 5)}
    xs = {d: (x + NX - d) % NX for d in range(-2, 3)}
    at = {
        "z+": (zs[-1] * NX + x) * 2 + core,
        "z-": (zs[1] * NX + x) * 2 + core,
        "x+": (z * NX + xs[-1]) * 2 + core,
        "x-": (z * NX + xs[1]) * 2 + core,
    }
    partner = chip * 2 + 1 - core
    y_up, y_down = (y + 1) % 4, (y + 3) % 4
    barrier = pltpu.get_barrier_semaphore()
    for dev in (*at.values(), partner):
        pl.semaphore_signal(barrier, inc=1, device_id={"sp": dev}, device_id_type=MESH)
    for dev in (y_up, y_down):
        pl.semaphore_signal(barrier, inc=1, device_id={"tp": dev}, device_id_type=MESH)

    pairs = [(freq_in, freq_ref), (k_in, k_ref), (kg_in, kg_ref)]
    pairs += [(v_in.at[pl.ds(h * 128, 128)], kv.at[h, :, pl.ds(128, 128)]) for h in (0, 1)]
    pairs += [(q_in, q_ref), (qg_in, qg_ref)]
    pairs += [(w, wbuf.at[2 * (NZ * NX * m + z * NX + x) + core]) for m, w in enumerate((gate_in, up_in, down_in))]
    pairs += [(wo_in, wo_ref), (res_in, res_ref), (ng_in, ng_ref)]
    loads = [pltpu.make_async_copy(a, b, in_sem.at[i]) for i, (a, b) in enumerate(pairs)]
    for load in loads:
        load.start()

    tok = q_ref.shape[0]
    heads = q_ref.shape[1] // 128
    rows = heads * tok
    scale = math.log2(math.e) / math.sqrt(128)
    lane = lax.broadcasted_iota(jnp.int32, (tok, 128), 1)
    token = lax.broadcasted_iota(jnp.int32, (tok, 128), 0) + me * tok
    place = jnp.where(lane < 64, token // GRID_W, token % GRID_W).astype(F32)
    for load in loads[:5]:
        load.wait()
    angle = place * freq_ref[...]
    cos_ref[...] = jnp.cos(angle)
    sin_ref[...] = jnp.sin(angle)
    k_rot = rope(k_ref[...].astype(F32), kg_ref[...], cos_ref[...], sin_ref[...], lane)
    for h in (0, 1):
        kv[h, :, 0:128] = k_rot[h * 128 : (h + 1) * 128]
    pl.semaphore_wait(barrier, 7)

    def send_on(slot):
        color, dz, dx = SLOTS[slot]
        for link, dz2, dx2 in next_hops(color, dz, dx):
            to = SLOT_OF[(color, dz2, dx2)]
            pltpu.make_async_remote_copy(
                kv.at[slot], kv.at[to], kv_send, kv_recv.at[to],
                device_id={"sp": at[link]}, device_id_type=MESH,
            ).start()

    def arrived(slot):
        pltpu.make_async_remote_copy(
            kv.at[slot], kv.at[slot], kv_send, kv_recv.at[slot],
            device_id={"sp": partner}, device_id_type=MESH,
        ).wait_recv()

    send_on(0)
    send_on(1)
    for load in loads[5:7]:
        load.wait()
    for h in range(heads):
        q_rot = rope(
            q_ref[:, h * 128 : (h + 1) * 128].astype(F32), qg_ref[...], cos_ref[...], sin_ref[...], lane
        )
        qall[rows + h * tok : rows + (h + 1) * tok, :] = q_rot

    def to_partner(src, dst, i):
        return pltpu.make_async_remote_copy(
            src, dst, swap_send.at[i], swap_recv.at[i], device_id={"sp": partner}, device_id_type=MESH
        )

    swap_q = to_partner(qall.at[pl.ds(rows, rows)], qall.at[pl.ds(0, rows)], 0)
    swap_acc = to_partner(acc.at[pl.ds(0, rows)], far_acc, 1)
    swap_top = to_partner(top.at[pl.ds(0, rows)], far_top, 2)
    swap_q.start()
    acc[...] = jnp.zeros_like(acc)
    top[...] = jnp.full_like(top, -1e30)
    for load in loads[7:]:
        load.wait()

    def weight_block(m, dz, dx):
        color = W_COLOR[m]
        block = wbuf.at[2 * (NZ * NX * m + zs[dz] * NX + xs[dx]) + core]
        n = W_INDEX[color][(dz, dx)]
        if (dz, dx) != (0, 0):
            pltpu.make_async_remote_copy(
                block, block, w_send, w_recv.at[m, n], device_id={"sp": partner}, device_id_type=MESH
            ).wait_recv()
        for link, dz2, dx2 in next_hops(color, dz, dx):
            pltpu.make_async_remote_copy(
                block, block, w_send, w_recv.at[m, W_INDEX[color][(dz2, dx2)]],
                device_id={"sp": at[link]}, device_id_type=MESH,
            ).start()
        pltpu.make_async_remote_copy(
            block, block, d2d_send, d2d_recv.at[m], device_id={"sp": partner}, device_id_type=MESH
        ).start()

    def weight_hop(ms, hop):
        for m in ms:
            for dz, dx in W_INDEX[W_COLOR[m]]:
                if abs(dz) + abs(dx) == hop:
                    weight_block(m, dz, dx)

    def attend(first, blocks):
        keys = kv[pl.ds(first, PER), :, 0:128].reshape(PER * 128, 128)
        vals = kv[pl.ds(first, PER), :, 128:256].reshape(PER * 128, 128)
        wide = jnp.concatenate([vals, jnp.ones((PER * 128, 128), BF16)], axis=1)
        for i in blocks:
            r = slice(i * BLOCK, (i + 1) * BLOCK)
            s = lax.dot_general(qall[r, :], keys, (((1,), (1,)), ((), ())), preferred_element_type=F32)
            old = top[r, :]
            new = jnp.maximum(old, jnp.max(s, axis=1, keepdims=True))
            top[r, :] = new
            shrink = jnp.exp2((old - new) * scale)
            w = jnp.exp2(s * scale - new[:, 0:1] * scale).astype(BF16)
            o = jnp.dot(w, wide, preferred_element_type=F32)
            acc[r, 0:128] = acc[r, 0:128] * shrink + o[:, 0:128]
            acc[r, 128:256] = acc[r, 128:256] * shrink + o[:, 128:256]

    def pass_on(k):
        for slot in range(max(2, PER * k), PER * (k + 1)):
            arrived(slot)
            send_on(slot)
        for ms, hop in W_AT_CHUNK.get(k, ()):
            weight_hop(ms, hop)

    def chunk(c, _):
        for k in range(1, N_SLOTS // PER - 1):

            @pl.when(c == k)
            def _():
                pass_on(k)

        attend(c * PER, range(2 * rows // BLOCK))
        return 0

    last = N_SLOTS // PER - 1
    pass_on(0)
    swap_q.wait_recv()
    lax.fori_loop(0, last, chunk, 0)
    pass_on(last)
    attend(last * PER, range(rows // BLOCK))
    swap_acc.start()
    swap_top.start()
    attend(last * PER, range(rows // BLOCK, 2 * rows // BLOCK))
    swap_acc.wait_recv()
    swap_top.wait_recv()
    for h in range(heads):
        mine = pl.ds(rows + h * tok, tok)
        far = pl.ds(h * tok, tok)
        t1, t2 = top[mine, :], far_top[far, :]
        t = jnp.maximum(t1, t2)
        a1, a2 = jnp.exp2((t1 - t) * scale), jnp.exp2((t2 - t) * scale)
        num = acc[mine, 0:128] * a1 + far_acc[far, 0:128] * a2
        den = acc[mine, 128:256] * a1 + far_acc[far, 128:256] * a2
        o = (num / den).astype(BF16)
        for j in range(4):
            att[(j + 4 - y) % 4, :, h * 128 : (h + 1) * 128] = o[j * 64 : (j + 1) * 64]

    def hop_y(src, dst, sems, i, dev):
        send, recv = sems
        return pltpu.make_async_remote_copy(
            src, dst, send.at[i], recv.at[i], device_id={"tp": dev}, device_id_type=MESH
        )

    def sum_over_tp(n, up, down, opposite):
        sems = (rs_send.at[n], rs_recv.at[n])
        t, p, s = terms.at[n], parts.at[n], sums.at[n]
        relay_up = hop_y(t.at[opposite, :, half(0)], p.at[0], sems, 0, y_up)
        relay_down = hop_y(t.at[opposite, :, half(1)], p.at[1], sems, 1, y_down)
        direct_up = hop_y(t.at[up, :, half(1)], p.at[2], sems, 2, y_up)
        direct_down = hop_y(t.at[down, :, half(0)], p.at[3], sems, 3, y_down)
        sum_up = hop_y(s.at[0], p.at[4], sems, 4, y_up)
        sum_down = hop_y(s.at[1], p.at[5], sems, 5, y_down)

        def first():
            relay_up.start()
            direct_down.start()

        def second():
            relay_down.start()
            direct_up.start()

        def third():
            relay_up.wait_recv()
            sums[n, 0] = (parts[n, 0].astype(F32) + terms[n, up, :, 0:1024].astype(F32)).astype(BF16)
            sum_up.start()
            relay_down.wait_recv()
            sums[n, 1] = (parts[n, 1].astype(F32) + terms[n, down, :, 1024:2048].astype(F32)).astype(BF16)
            sum_down.start()

        def total():
            direct_down.wait_recv()
            direct_up.wait_recv()
            sum_up.wait_recv()
            sum_down.wait_recv()
            low = terms[n, 0, :, 0:1024].astype(F32) + parts[n, 3].astype(F32) + parts[n, 4].astype(F32)
            high = terms[n, 0, :, 1024:2048].astype(F32) + parts[n, 2].astype(F32) + parts[n, 5].astype(F32)
            return jnp.concatenate([low, high], axis=1)

        def sent():
            for c in (relay_up, relay_down, direct_up, direct_down, sum_up, sum_down):
                c.wait_send()

        return first, second, third, total, sent

    first, second, third, total, sent = sum_over_tp(0, 1, 3, 2)
    lhs = att[...].reshape(tok, heads * 128)
    for k, go in ((0, first), (1, second)):
        piece = jnp.dot(lhs, wo_ref[:, k * 1024 : (k + 1) * 1024], preferred_element_type=F32)
        terms[0, :, :, k * 1024 : (k + 1) * 1024] = piece.astype(BF16).reshape(4, 64, 1024)
        go()
    for ms, hop in W_AFTER["projected"]:
        weight_hop(ms, hop)
    third()
    for ms, hop in W_AFTER["relayed"]:
        weight_hop(ms, hop)
    mixed = (res_ref[...].astype(F32) + total()).astype(BF16)
    res_ref[...] = mixed
    mixed_f = mixed.astype(F32)
    normed = mixed_f * lax.rsqrt(jnp.mean(mixed_f * mixed_f, axis=-1, keepdims=True) + EPS) * ng_ref[...]
    rows_ref[0] = normed.astype(BF16)

    ag = (ag_send, ag_recv)
    own_up = [hop_y(rows_ref.at[0, :, half(k)], rows_ref.at[1, :, half(k)], ag, k, y_up) for k in (0, 1)]
    own_down = [hop_y(rows_ref.at[0, :, half(k)], rows_ref.at[2, :, half(k)], ag, 2 + k, y_down) for k in (0, 1)]
    on_up = hop_y(rows_ref.at[1, :, half(0)], rows_ref.at[3, :, half(0)], ag, 4, y_up)
    on_down = hop_y(rows_ref.at[2, :, half(1)], rows_ref.at[3, :, half(1)], ag, 5, y_down)
    own_up[0].start()
    own_down[1].start()
    own_up[1].start()
    own_down[0].start()
    for ms, hop in W_AFTER["normed"]:
        weight_hop(ms, hop)
    own_up[0].wait_recv()
    on_up.start()
    own_down[1].wait_recv()
    on_down.start()
    for ms, hop in W_AFTER["passed"]:
        weight_hop(ms, hop)
    for c in (own_up[1], own_down[0], on_up, on_down):
        c.wait_recv()

    def from_partner(m):
        whole = wbuf.at[pl.ds(0, NZ * NX)]
        return pltpu.make_async_remote_copy(
            whole, whole, d2d_send, d2d_recv.at[m], device_id={"sp": partner}, device_id_type=MESH
        )

    from_partner(0).wait_recv()
    from_partner(1).wait_recv()
    units = hidden.shape[1]
    for n in range(units // 128):
        cols = slice(n * 128, (n + 1) * 128)
        both = jnp.concatenate(
            [wbuf[64 * m : 64 * (m + 1), :, cols].reshape(NZ * NX * 64, 128) for m in (0, 1)], axis=1
        )
        gu = jnp.dot(rows_ref[...].reshape(tok, NZ * NX * 64), both, preferred_element_type=F32)
        gate, up = gu[:, 0:128], gu[:, 128:256]
        hidden[:, cols] = (gate / (1.0 + jnp.exp(-gate)) * up).astype(BF16)
        for ms, hop in W_IN_FFN.get(n, ()):
            weight_hop(ms, hop)
    from_partner(2).wait_recv()
    first, second, third, total, sent2 = sum_over_tp(1, 2, 1, 3)
    for k in range(NZ):
        piece = lax.dot_general(
            hidden[...], wbuf[128 + 8 * k : 136 + 8 * k].reshape(256, units), (((1,), (1,)), ((), ())), preferred_element_type=F32
        )
        terms[1, :, :, k * 256 : (k + 1) * 256] = piece.astype(BF16).reshape(4, 64, 256)
        if k == NZ // 2 - 1:
            first()
    second()
    third()
    out_ref[...] = (res_ref[...].astype(F32) + 0.5 * total()).astype(BF16)

    moved = kv.at[pl.ds(0, N_SLOTS - 2)]
    pltpu.make_async_remote_copy(
        moved, moved, kv_send, kv_recv.at[0], device_id={"sp": partner}, device_id_type=MESH
    ).wait_send()
    for blocks, sem in ((3 * (NZ * NX - 1), w_send), (3 * NZ * NX, d2d_send)):
        moved = wbuf.at[pl.ds(0, blocks)]
        pltpu.make_async_remote_copy(
            moved, moved, sem, d2d_recv.at[0], device_id={"sp": partner}, device_id_type=MESH
        ).wait_send()
    for c in (swap_q, swap_acc, swap_top, *own_up, *own_down, on_up, on_down):
        c.wait_send()
    sent()
    sent2()


W_COLOR = (0, 1, 0)
W_INDEX = [{b: i for i, b in enumerate(blocks_of(color))} for color in (0, 1)]
GU, DOWN = (0, 1), (2,)
W_AT_CHUNK = {1: [(GU, 0)], 3: [(GU, 1)], 5: [(GU, 2)], 7: [(GU, 3)]}
W_AFTER = {
    "projected": [(GU, 4), (DOWN, 0)],
    "relayed": [(GU, 5), (DOWN, 1)],
    "normed": [(GU, 6), (DOWN, 2)],
    "passed": [(DOWN, 3)],
}
W_IN_FFN = {2: [(DOWN, 4)], 5: [(DOWN, 5)], 8: [(DOWN, 6)]}


def per_device(
    residual_in,
    queries,
    keys_raw,
    values_raw,
    query_gain,
    key_gain,
    out_weight,
    norm_gain,
    gate_weight,
    up_weight,
    down_weight,
):
    tok, width = queries.shape
    rows = tok * width // 128
    d = residual_in.shape[1]
    units = gate_weight.shape[1]
    freq = (THETA ** (-np.arange(0, 64, 2, dtype=np.float64) / 64)).astype(np.float32)
    freq = jnp.asarray(np.tile(freq, 4)[None])
    dma = pltpu.SemaphoreType.DMA
    return pl.pallas_call(
        layer_kernel,
        out_shape=jax.ShapeDtypeStruct(residual_in.shape, BF16),
        in_specs=[pl.BlockSpec(memory_space=pl.ANY)] * 12,
        out_specs=pl.BlockSpec(memory_space=pltpu.VMEM),
        scratch_shapes=[
            pltpu.VMEM((N_SLOTS, 128, 256), BF16),
            pltpu.VMEM((2 * rows, 128), BF16),
            pltpu.VMEM((2 * rows, 256), F32),
            pltpu.VMEM((2 * rows, 128), F32),
            pltpu.VMEM((rows, 256), F32),
            pltpu.VMEM((rows, 128), F32),
            pltpu.VMEM((tok, 128), F32),
            pltpu.VMEM((tok, 128), F32),
            pltpu.VMEM(residual_in.shape, BF16),
            pltpu.VMEM(queries.shape, BF16),
            pltpu.VMEM(keys_raw.shape, BF16),
            pltpu.VMEM((1, 128), F32),
            pltpu.VMEM((1, 128), F32),
            pltpu.VMEM(out_weight.shape, BF16),
            pltpu.VMEM((1, d), F32),
            pltpu.VMEM((1, 128), F32),
            pltpu.VMEM((3 * NZ * NX * 2, 32, units), BF16),
            pltpu.VMEM((4, tok // 4, width), BF16),
            pltpu.VMEM((2, 4, tok // 4, d), BF16),
            pltpu.VMEM((2, 2, tok // 4, d // 2), BF16),
            pltpu.VMEM((2, 6, tok // 4, d // 2), BF16),
            pltpu.VMEM((4, tok // 4, d), BF16),
            pltpu.VMEM((tok, units), BF16),
            dma((13,)),
            dma((N_SLOTS,)),
            dma,
            dma((3,)),
            dma((3,)),
            dma((3, NZ * NX)),
            dma,
            dma((3,)),
            dma,
            dma((2, 6)),
            dma((2, 6)),
            dma((6,)),
            dma((6,)),
        ],
        compiler_params=pltpu.CompilerParams(
            collective_id=0, has_side_effects=True, vmem_limit_bytes=60 * 2**20
        ),
    )(
        residual_in, queries, keys_raw, values_raw, query_gain[None], key_gain[None], out_weight,
        norm_gain[None], gate_weight, up_weight, down_weight.T, freq,
    )


def solution(mesh):
    placed = (
        P(("sp", "tp"), None),
        P("sp", "tp"),
        P("sp", "tp"),
        P("sp", "tp"),
        P(),
        P(),
        P("tp", None),
        P(),
        P("sp", "tp"),
        P("sp", "tp"),
        P("tp", "sp"),
    )
    return jax.shard_map(
        per_device, mesh=mesh, in_specs=placed, out_specs=P(("sp", "tp"), None), check_vma=False
    )
```

time: 177 us -> 117 us (0.66); the launches traced: 175 us -> 117 us
  blocking collectives: 49.6 us -> 0 us
  Pallas kernels: 88.5 us -> 115 us
  matrix products: 15.4 us -> 0 us
  between operations: 13.5 us -> 0.01 us
  other arithmetic: 3.27 us -> 0 us
  local copies, waits for them, and re-layouts: 4.71 us -> 1.67 us
    all_to_all x3 -> x0, blocking collectives: 49.6 us -> none  [the longest x2 33.8 us: sent_and_summed(): pieces = lax.all_to_all(in_blocks(x, dim, length), axis, 0, 0, tiled=True)]
    pallas_call x1, Pallas kernels: 88.5 us -> 115 us  [per_device(): pl.pallas_call(layer_kernel, out_shape=jax.ShapeDtypeStruct(residual_in.s...]
    dot_general x3 -> x0, matrix products: 15.4 us -> none  [the longest x1 9.17 us: per_device(): lax.dot_general(hidden, weights[:, 2 * units:], (((1,), (1,)), ((), ())),...]
    unnamed x18 -> x1, local copies, waits for them, and re-layouts: 4.6 us -> 1.67 us
    concatenate x1 -> x0, other arithmetic: 1.86 us -> none  [per_device(): weights = jnp.concatenate([gate_weight, up_weight, down_weight.T], axis=1)]
  transfers between devices with their start and end apart: 1 -> 0, of which waited for: 0 -> 0; matrix products, arithmetic and copies ran while one was open for 1% -> 0% of each run, Pallas kernels for 51% -> 0%
where the time goes in v2:
time: 117 us
  Pallas kernels  115 us (98%)
  local copies, waits for them, and re-layouts  1.67 us (1%)
    pallas_call x1, Pallas kernels, per_device(): pl.pallas_call(layer_kernel, out_shape=jax.ShapeDtypeStruct(residual_in.s...  115 us

profile of v2, /device:TPU:1, one launch (start us, length us, event | category | flops | bytes accessed | tf_op | source)
XLA Modules:
  0.0 117.1 jit_solution(5460732477515029079)
XLA Ops:
  0.0 115.4 %shard_map.118 = bf16[64,2048]{1,0:T(8,128)(2,1)} custom-call(bf16[64,2048]{1,0:T(8,128)(2,1)} %res_in.1, bf16[256,512]{1,0:T(8,128)(2,1)} %q_in.1, bf16[256,128]{1,0:T(8,128)(2,1)} %k_in.1, bf16[256,128]{1,0:T(8,128)(2,1)} %v_in.1, f32[1,128]{1,0:T(1,128)} %bitcast.6, f32[1,128]{1,0:T(1,128)} %bitcast.7, bf16[512,2048]{1,0:T(8,128)(2,1)} %wo_in.1, ...), custom_call_target="tpu_custom_call" | custom-call | tf_op jit(solution)/shard_map/pallas_call | solution.py:422
  115.4 1.7 %copy.14 = bf16[64,2048]{1,0:T(8,128)(2,1)} copy(bf16[64,2048]{1,0:T(8,128)(2,1)} %shard_map.118) | data formatting | bytes 524288

commit v3 on v2

v3 whole, which is shorter than its diff:
```python
import math

import jax
import jax.numpy as jnp
import numpy as np
from jax import lax
from jax.experimental import pallas as pl
from jax.experimental.pallas import tpu as pltpu
from jax.sharding import PartitionSpec as P

GRID_W = 64
EPS = 1e-06
THETA = 10000.0
MESH = pl.DeviceIdType.MESH
NZ, NX = 8, 4
F32 = jnp.float32
BF16 = jnp.bfloat16


MIRROR = {"z+": "z-", "z-": "z+", "x+": "x-", "x-": "x+"}


def next_hops(color, dz, dx):
    if color >= 2:
        return [(MIRROR[link], -a, -b) for link, a, b in next_hops(color - 2, -dz, -dx)]
    out = []
    if color == 0:
        if dx == 0:
            if 0 <= dz < 4:
                out.append(("z+", dz + 1, 0))
            if -3 < dz <= 0:
                out.append(("z-", dz - 1, 0))
            out.append(("x+", dz, 1))
            out.append(("x-", dz, -1))
        elif dx == 1 and dz % 2 == 0:
            out.append(("x+", dz, 2))
        elif dx == -1 and dz % 2 == 1:
            out.append(("x-", dz, -2))
    else:
        if dz == 0:
            if dx == 0:
                out.append(("x+", 0, 1))
                out.append(("x-", 0, -1))
            elif dx == 1:
                out.append(("x+", 0, 2))
            out.append(("z+", 1, dx))
            out.append(("z-", -1, dx))
        elif dz > 0:
            if dz < (4 if dx % 2 == 0 else 3):
                out.append(("z+", dz + 1, dx))
        else:
            if -dz < (3 if dx % 2 == 0 else 4):
                out.append(("z-", dz - 1, dx))
    return out


def blocks_of(color):
    seen, todo = [], [(0, 0)]
    while todo:
        at = todo.pop(0)
        seen.append(at)
        todo += [(dz, dx) for _, dz, dx in next_hops(color, *at)]
    assert len(seen) == NZ * NX and len({(dz % NZ, dx % NX) for dz, dx in seen}) == NZ * NX
    return seen


W_COLOR = (3, 2, 2)
SCHEDULE = {
    'start': [
        (3, 0, 0), (4, 0, 0),
    ],
    'chunk0': [
        (0, 0, 0), (1, 0, 0), (2, 0, 0), (3, 1, 0), (3, -1, 0), (3, 0, 1), (3, 0, -1), (4, 1, 0), (4, -1, 0),
        (5, 0, 0), (4, 0, 1), (5, 1, 0), (4, 0, -1),
    ],
    'chunk1': [
        (1, 0, 1), (1, 0, -1), (0, 1, 0), (0, -1, 0), (2, 0, 1), (2, 0, -1), (3, 2, 0), (3, -2, 0), (3, 1, 1),
        (3, 1, -1), (4, 2, 0), (4, -2, 0), (3, -1, 1), (3, -1, -1),
    ],
    'chunk2': [
        (4, 1, 1), (4, -1, 1), (3, 0, 2), (4, 1, -1), (4, -1, -1), (4, 0, 2), (1, 0, -2),
    ],
    'chunk3': [
        (5, 2, 0), (5, 3, 0), (3, 2, 1), (3, 2, -1), (3, -2, 1), (3, 3, 0), (3, -3, 0), (0, -2, 0),
        (2, 0, -2), (3, -2, -1), (0, 2, 0), (4, 3, 0), (4, -3, 0),
    ],
    'chunk4': [
        (3, 1, -2), (4, 2, 1), (4, -2, 1), (3, -1, -2), (3, 2, 2), (4, 2, -1), (4, -2, -1), (1, -1, 0),
        (3, 3, -1),
    ],
    'chunk5': [
        (3, -2, 2), (4, 1, 2), (4, -1, 2), (3, -3, -1), (3, 3, 1), (3, 4, 0), (3, -3, 1), (0, -3, 0),
        (1, -1, -1), (1, 1, 0), (4, -3, 1), (0, 3, 0),
    ],
    'chunk6': [
        (3, 3, -2), (4, 4, 0), (4, -3, -1), (3, 4, 1), (3, -3, -2), (4, 3, 1), (1, -1, 1), (2, 1, 0),
        (0, 0, 1), (3, 4, -1), (4, 3, -1),
    ],
    'chunk7': [
        (4, -2, 2), (4, 2, 2), (3, 4, 2), (0, 0, -1), (1, 1, 1), (1, 1, -1), (0, -4, 0), (2, 1, -1),
        (4, -4, 1), (1, -1, 2), (1, -2, 0), (1, 2, 0), (4, -4, -1), (2, 1, 1), (0, 0, -2), (1, 1, 2),
        (4, 3, 2), (4, -3, 2), (0, -1, 1), (1, -2, -1), (0, 1, 1), (1, -2, 1), (2, -1, 0), (1, 2, -1),
        (0, 1, -1), (1, 2, 1), (0, -1, -1), (1, 3, 0), (1, -2, -2), (2, 2, 0), (2, 1, 2), (0, -1, -2),
        (2, -1, -1), (4, 4, 2), (1, -3, 0), (0, 1, -2), (2, -1, 1),
    ],
    'chunk8': [
        (0, -2, 1), (1, 2, -2), (0, 2, 1), (1, 3, 1), (1, 3, -1),
    ],
    'att': [
        (0, 2, -1), (0, -2, -1), (2, 2, 1), (2, 2, -1),
    ],
    'own': [
        (1, -3, 1), (2, 3, 0), (0, -2, -2), (1, -3, -1), (0, 2, -2), (2, -1, 2), (1, -4, 0), (2, 2, -2),
        (0, 3, 1), (2, -2, 0), (1, 3, 2),
    ],
    'relay': [
        (0, -3, 1), (2, 3, -1), (0, 3, -1), (1, -3, 2), (0, -3, -1),
    ],
    'two': [
        (1, -4, -1), (0, 3, -2), (0, -3, -2), (2, 3, 1), (2, -2, -1), (0, 4, 1), (1, -4, 1),
    ],
    'opp': [
        (2, -3, 0), (0, 4, -1), (2, -2, 1), (1, -4, -2), (0, -4, -2),
    ],
    'ffn0': [
        (2, 3, 2),
    ],
    'ffn1': [
        (2, -2, -2),
    ],
    'ffn4': [
        (2, -4, 0), (2, -3, 1),
    ],
    'ffn5': [
        (2, -3, -1),
    ],
    'plane3': [
        (2, -4, -1), (2, -4, 1),
    ],
    'plane4': [
        (2, -3, 2),
    ],
    'plane6': [
        (2, -4, -2),
    ],
}
SLOTS = [(what - 3, dz, dx) for events in SCHEDULE.values() for what, dz, dx in events if what in (3, 4)]
SLOT_OF = {b: i for i, b in enumerate(SLOTS)}
N_SLOTS = len(SLOTS)
PER = 8
PLANES = (0, 1, -1, 2, -2, 3, -3, 4)
LAG = 3
BLOCK = 128


W_INDEX = [{b: i for i, b in enumerate(blocks_of(color))} for color in W_COLOR]


def rope(v, gain, cos, sin, lane):
    v = v * lax.rsqrt(jnp.mean(v * v, axis=-1, keepdims=True) + EPS) * gain
    turned = jnp.where(lane % 64 < 32, -pltpu.roll(v, 96, 1), pltpu.roll(v, 32, 1))
    return (v * cos + turned * sin).astype(BF16)


def layer_kernel(
    res_in, q_in, k_in, v_in, qg_in, kg_in, wo_in, ng_in, gate_in, up_in, down_in, freq_in, out_ref,
    kv, qall, acc, top, far_acc, far_top, cos_ref, sin_ref,
    res_ref, q_ref, k_ref, qg_ref, kg_ref, wo_ref, ng_ref, freq_ref,
    wbuf, att, proj, mix, rows_ref, hidden, terms, sums, parts,
    in_sem, kv_recv, kv_send, swap_recv, swap_send,
    w_recv, w_send, d2d_recv, d2d_send, ring_recv, ring_send, wo_recv, wo_send, rs_recv, rs_send,
):
    me = lax.axis_index("sp")
    y = lax.axis_index("tp")
    core = me % 2
    chip = me // 2
    x = chip % NX
    z = chip // NX
    zs = {d: (z + NZ - d) % NZ for d in range(-4, 5)}
    xs = {d: (x + NX - d) % NX for d in range(-2, 3)}
    at = {
        "z+": (zs[-1] * NX + x) * 2 + core,
        "z-": (zs[1] * NX + x) * 2 + core,
        "x+": (z * NX + xs[-1]) * 2 + core,
        "x-": (z * NX + xs[1]) * 2 + core,
    }
    partner = chip * 2 + 1 - core
    y_up, y_down, y_far = (y + 1) % 4, (y + 3) % 4, (y + 2) % 4
    barrier = pltpu.get_barrier_semaphore()
    for dev in (*at.values(), partner):
        pl.semaphore_signal(barrier, inc=1, device_id={"sp": dev}, device_id_type=MESH)
    for dev in (y_up, y_down):
        pl.semaphore_signal(barrier, inc=1, device_id={"tp": dev}, device_id_type=MESH)

    pairs = [(freq_in, freq_ref), (k_in, k_ref), (kg_in, kg_ref)]
    pairs += [(v_in.at[pl.ds(h * 128, 128)], kv.at[h, :, pl.ds(128, 128)]) for h in (0, 1)]
    pairs += [(q_in, q_ref), (qg_in, qg_ref)]
    pairs += [(res_in, res_ref.at[y])]
    pairs += [(wo_in.at[pl.ds(h * 256, 256)], wo_ref.at[0, h]) for h in (0, 1)]
    pairs += [(w, wbuf.at[2 * (NZ * NX * m + z * NX + x) + core]) for m, w in enumerate((gate_in, up_in, down_in))]
    pairs += [(ng_in, ng_ref)]
    loads = [pltpu.make_async_copy(a, b, in_sem.at[i]) for i, (a, b) in enumerate(pairs)]
    for load in loads:
        load.start()

    tok = q_ref.shape[0]
    heads = q_ref.shape[1] // 128
    rows = heads * tok
    scale = math.log2(math.e) / math.sqrt(128)
    lane = lax.broadcasted_iota(jnp.int32, (tok, 128), 1)
    token = lax.broadcasted_iota(jnp.int32, (tok, 128), 0) + me * tok
    place = jnp.where(lane < 64, token // GRID_W, token % GRID_W).astype(F32)
    for load in loads[:5]:
        load.wait()
    angle = place * freq_ref[...]
    cos_ref[...] = jnp.cos(angle)
    sin_ref[...] = jnp.sin(angle)
    k_rot = rope(k_ref[...].astype(F32), kg_ref[...], cos_ref[...], sin_ref[...], lane)
    for h in (0, 1):
        kv[h, :, 0:128] = k_rot[h * 128 : (h + 1) * 128]
    pl.semaphore_wait(barrier, 7)

    def send_on(slot):
        color, dz, dx = SLOTS[slot]
        for link, dz2, dx2 in next_hops(color, dz, dx):
            to = SLOT_OF[(color, dz2, dx2)]
            pltpu.make_async_remote_copy(
                kv.at[slot], kv.at[to], kv_send, kv_recv.at[to],
                device_id={"sp": at[link]}, device_id_type=MESH,
            ).start()

    def arrived(slot):
        pltpu.make_async_remote_copy(
            kv.at[slot], kv.at[slot], kv_send, kv_recv.at[slot],
            device_id={"sp": partner}, device_id_type=MESH,
        ).wait_recv()

    def gather_y(n, ref, own, below, above, slot_up, slot_down, far_up, far_down, piece):
        def hop(i, src, dst, k, dev):
            return pltpu.make_async_remote_copy(
                ref.at[src, *piece(k)], ref.at[dst, *piece(k)], ring_send.at[n, i], ring_recv.at[n, i],
                device_id={"tp": dev}, device_id_type=MESH,
            )

        return (
            [hop(k, own, slot_up, k, y_up) for k in (0, 1)],
            [hop(2 + k, own, slot_down, k, y_down) for k in (0, 1)],
            hop(4, below, far_up, 0, y_up),
            hop(5, above, far_down, 1, y_down),
        )

    def begin(ring):
        ups, downs, _, _ = ring
        ups[0].start()
        downs[1].start()
        ups[1].start()
        downs[0].start()

    res_ring = gather_y(0, res_ref, y, y_down, y_up, y, y, y_down, y_up, lambda k: (pl.ds(32 * k, 32),))
    wo_ring = gather_y(1, wo_ref, 0, 1, 2, 1, 2, 3, 3, lambda k: (core, pl.ds(128 * k, 128)))
    att_ring = gather_y(2, att, 0, 1, 2, 1, 2, 3, 3, lambda k: (pl.ds(128 * k, 128),))

    def wo_to_partner(slot, k):
        piece = wo_ref.at[slot, core, pl.ds(128 * k, 128)]
        pltpu.make_async_remote_copy(
            piece, piece, wo_send, wo_recv, device_id={"sp": partner}, device_id_type=MESH
        ).start()

    def pass_round(code):
        ring = (res_ring, wo_ring)[code // 2]
        if code % 2 == 0:
            ring[0][0].wait_recv()
            ring[2].start()
        else:
            ring[1][1].wait_recv()
            ring[3].start()
        if code >= 2:
            wo_to_partner(1 + code % 2, code % 2)

    send_on(0)
    send_on(1)
    for load in loads[7:10]:
        load.wait()
    begin(res_ring)
    begin(wo_ring)
    for load in loads[5:7]:
        load.wait()
    for h in range(heads):
        q_rot = rope(
            q_ref[:, h * 128 : (h + 1) * 128].astype(F32), qg_ref[...], cos_ref[...], sin_ref[...], lane
        )
        qall[rows + h * tok : rows + (h + 1) * tok, :] = q_rot

    def to_partner(src, dst, i):
        return pltpu.make_async_remote_copy(
            src, dst, swap_send.at[i], swap_recv.at[i], device_id={"sp": partner}, device_id_type=MESH
        )

    swap_q = to_partner(qall.at[pl.ds(rows, rows)], qall.at[pl.ds(0, rows)], 0)
    swap_acc = to_partner(acc.at[pl.ds(0, rows)], far_acc, 1)
    swap_top = to_partner(top.at[pl.ds(0, rows)], far_top, 2)
    swap_q.start()
    acc[...] = jnp.zeros_like(acc)
    top[...] = jnp.full_like(top, -1e30)
    for load in loads[10:]:
        load.wait()

    def weight_block(m, dz, dx):
        color = W_COLOR[m]
        block = wbuf.at[2 * (NZ * NX * m + zs[dz] * NX + xs[dx]) + core]
        n = W_INDEX[m][(dz, dx)]
        if (dz, dx) != (0, 0):
            pltpu.make_async_remote_copy(
                block, block, w_send, w_recv.at[m, n], device_id={"sp": partner}, device_id_type=MESH
            ).wait_recv()
        for link, dz2, dx2 in next_hops(color, dz, dx):
            pltpu.make_async_remote_copy(
                block, block, w_send, w_recv.at[m, W_INDEX[m][(dz2, dx2)]],
                device_id={"sp": at[link]}, device_id_type=MESH,
            ).start()
        pltpu.make_async_remote_copy(
            block, block, d2d_send, d2d_recv.at[m + (dz % NZ if m == 2 else 0)], device_id={"sp": partner}, device_id_type=MESH
        ).start()

    def events(point):
        for what, dz, dx in SCHEDULE.get(point, ()):
            if what == 5:
                pass_round(dz)
            elif what >= 3:
                slot = SLOT_OF[(what - 3, dz, dx)]
                if slot >= 2:
                    arrived(slot)
                    send_on(slot)
            else:
                weight_block(what, dz, dx)

    def attend(first, blocks):
        keys = kv[pl.ds(first, PER), :, 0:128].reshape(PER * 128, 128)
        vals = kv[pl.ds(first, PER), :, 128:256].reshape(PER * 128, 128)
        wide = jnp.concatenate([vals, jnp.ones((PER * 128, 128), BF16)], axis=1)
        for i in blocks:
            r = slice(i * BLOCK, (i + 1) * BLOCK)
            s = lax.dot_general(qall[r, :], keys, (((1,), (1,)), ((), ())), preferred_element_type=F32)
            old = top[r, :]
            new = jnp.maximum(old, jnp.max(s, axis=1, keepdims=True))
            top[r, :] = new
            shrink = jnp.exp2((old - new) * scale)
            w = jnp.exp2(s * scale - new[:, 0:1] * scale).astype(BF16)
            o = jnp.dot(w, wide, preferred_element_type=F32)
            acc[r, 0:128] = acc[r, 0:128] * shrink + o[:, 0:128]
            acc[r, 128:256] = acc[r, 128:256] * shrink + o[:, 128:256]

    def chunk(c, _):
        for k in range(1, N_SLOTS // PER - 1):

            @pl.when(c == k)
            def _():
                events(f"chunk{k}")

        attend(c * PER, range(2 * rows // BLOCK))
        return 0

    last = N_SLOTS // PER - 1
    events("chunk0")
    swap_q.wait_recv()
    lax.fori_loop(0, last, chunk, 0)
    events(f"chunk{last}")
    wo_ring[0][1].wait_recv()
    wo_to_partner(1, 1)
    wo_ring[1][0].wait_recv()
    wo_to_partner(2, 0)
    attend(last * PER, range(rows // BLOCK))
    swap_acc.start()
    swap_top.start()
    attend(last * PER, range(rows // BLOCK, 2 * rows // BLOCK))
    events(f"chunk{last + 1}")
    swap_acc.wait_recv()
    swap_top.wait_recv()
    for h in range(heads):
        mine = pl.ds(rows + h * tok, tok)
        far = pl.ds(h * tok, tok)
        t1, t2 = top[mine, :], far_top[far, :]
        t = jnp.maximum(t1, t2)
        a1, a2 = jnp.exp2((t1 - t) * scale), jnp.exp2((t2 - t) * scale)
        num = acc[mine, 0:128] * a1 + far_acc[far, 0:128] * a2
        den = acc[mine, 128:256] * a1 + far_acc[far, 128:256] * a2
        att[0, :, h * 128 : (h + 1) * 128] = (num / den).astype(BF16)

    def group_term(g):
        term = jnp.dot(att[g], wo_ref[g].reshape(2 * tok, NZ * NX * 64), preferred_element_type=F32)
        return term.astype(BF16).astype(F32)

    begin(att_ring)
    events("att")
    proj[...] = group_term(0)
    events("own")
    att_ring[0][0].wait_recv()
    att_ring[2].start()
    att_ring[1][1].wait_recv()
    att_ring[3].start()
    events("relay")
    for k, (slot, c) in enumerate(((3, wo_ring[2]), (3, wo_ring[3]))):
        c.wait_recv()
        wo_to_partner(slot, k)
    shared = wo_ref.at[pl.ds(1, 3), 1 - core]
    from_other = pltpu.make_async_remote_copy(
        shared, shared, wo_send, wo_recv, device_id={"sp": partner}, device_id_type=MESH
    )
    from_other.wait_recv()
    att_ring[0][1].wait_recv()
    proj[...] += group_term(1)
    att_ring[1][0].wait_recv()
    proj[...] += group_term(2)
    events("two")
    for c in (res_ring[0][0], res_ring[0][1], res_ring[1][0], res_ring[1][1], res_ring[2], res_ring[3]):
        if c is not res_ring[0][0] and c is not res_ring[1][1]:
            c.wait_recv()
    att_ring[2].wait_recv()
    att_ring[3].wait_recv()
    proj[...] += group_term(3)
    for j in range(4):
        r = slice(64 * j, 64 * (j + 1))
        mixed = (res_ref[j].astype(F32) + proj[r]).astype(BF16)
        mix[j] = mixed
        mixed_f = mixed.astype(F32)
        normed = mixed_f * lax.rsqrt(jnp.mean(mixed_f * mixed_f, axis=-1, keepdims=True) + EPS) * ng_ref[...]
        rows_ref[r] = normed.astype(BF16)
    events("opp")

    def from_partner(i, blocks):
        whole = wbuf.at[pl.ds(0, blocks)]
        return pltpu.make_async_remote_copy(
            whole, whole, d2d_send, d2d_recv.at[i], device_id={"sp": partner}, device_id_type=MESH
        )

    from_partner(0, NZ * NX).wait_recv()
    from_partner(1, NZ * NX).wait_recv()
    events("ffn0")
    units = hidden.shape[1]
    for n in range(units // 128):
        cols = slice(n * 128, (n + 1) * 128)
        both = jnp.concatenate(
            [wbuf[64 * m : 64 * (m + 1), :, cols].reshape(NZ * NX * 64, 128) for m in (0, 1)], axis=1
        )
        gu = jnp.dot(rows_ref[...], both, preferred_element_type=F32)
        gate, up = gu[:, 0:128], gu[:, 128:256]
        hidden[:, cols] = (gate / (1.0 + jnp.exp(-gate)) * up).astype(BF16)
        events(f"ffn{n + 1}")

    def plane_copies(i):
        def hop(n, src, dev):
            return pltpu.make_async_remote_copy(
                src, parts.at[i, n], rs_send.at[i, n], rs_recv.at[i, n],
                device_id={"tp": dev}, device_id_type=MESH,
            )

        low, high = pl.ds(0, 32), pl.ds(32, 32)
        return [
            hop(0, terms.at[i, y_far, low], y_up),
            hop(1, terms.at[i, y_far, high], y_down),
            hop(2, terms.at[i, y_up, high], y_up),
            hop(3, terms.at[i, y_down, low], y_down),
            hop(4, sums.at[i, 0], y_up),
            hop(5, sums.at[i, 1], y_down),
        ]

    copies = [plane_copies(i) for i in range(NZ)]

    def add_and_pass(i):
        copies[i][0].wait_recv()
        sums[i, 0] = (parts[i, 0].astype(F32) + terms[i, y_up, 0:32].astype(F32)).astype(BF16)
        copies[i][4].start()
        copies[i][1].wait_recv()
        sums[i, 1] = (parts[i, 1].astype(F32) + terms[i, y_down, 32:64].astype(F32)).astype(BF16)
        copies[i][5].start()

    for i, dz in enumerate(PLANES):
        from_partner(2 + dz % NZ, NX).wait_recv()
        rhs = wbuf[pl.ds(2 * NZ * NX * 2 + 8 * zs[dz], 8)].reshape(256, units)
        piece = lax.dot_general(hidden[...], rhs, (((1,), (1,)), ((), ())), preferred_element_type=F32)
        terms[i] = piece.astype(BF16).reshape(4, 64, 256)
        for c in copies[i][:4]:
            c.start()
        events(f"plane{i}")
        if i >= LAG:
            add_and_pass(i - LAG)
    for i in range(NZ - LAG, NZ):
        add_and_pass(i)
    for i, dz in enumerate(PLANES):
        for c in copies[i][2:]:
            c.wait_recv()
        cols = pl.ds(pl.multiple_of(256 * zs[dz], 256), 256)
        for h, (a, b) in enumerate(((3, 4), (2, 5))):
            r = slice(32 * h, 32 * (h + 1))
            fed = terms[i, y, r].astype(F32) + parts[i, a].astype(F32) + parts[i, b].astype(F32)
            out_ref[r, cols] = (mix[y, r, cols].astype(F32) + 0.5 * fed).astype(BF16)

    moved = kv.at[pl.ds(0, N_SLOTS - 2)]
    pltpu.make_async_remote_copy(
        moved, moved, kv_send, kv_recv.at[0], device_id={"sp": partner}, device_id_type=MESH
    ).wait_send()
    for blocks, sem in ((3 * (NZ * NX - 1), w_send), (3 * NZ * NX, d2d_send)):
        moved = wbuf.at[pl.ds(0, blocks)]
        pltpu.make_async_remote_copy(
            moved, moved, sem, d2d_recv.at[0], device_id={"sp": partner}, device_id_type=MESH
        ).wait_send()
    for ups, downs, a, b in (res_ring, wo_ring, att_ring):
        for c in (*ups, *downs, a, b):
            c.wait_send()
    for c in (swap_q, swap_acc, swap_top, from_other):
        c.wait_send()
    for plane in copies:
        for c in plane:
            c.wait_send()


def per_device(
    residual_in,
    queries,
    keys_raw,
    values_raw,
    query_gain,
    key_gain,
    out_weight,
    norm_gain,
    gate_weight,
    up_weight,
    down_weight,
):
    tok, width = queries.shape
    rows = tok * width // 128
    d = residual_in.shape[1]
    units = gate_weight.shape[1]
    freq = (THETA ** (-np.arange(0, 64, 2, dtype=np.float64) / 64)).astype(np.float32)
    freq = jnp.asarray(np.tile(freq, 4)[None])
    dma = pltpu.SemaphoreType.DMA
    return pl.pallas_call(
        layer_kernel,
        out_shape=jax.ShapeDtypeStruct(residual_in.shape, BF16),
        in_specs=[pl.BlockSpec(memory_space=pl.ANY)] * 12,
        out_specs=pl.BlockSpec(memory_space=pltpu.VMEM),
        scratch_shapes=[
            pltpu.VMEM((N_SLOTS, 128, 256), BF16),
            pltpu.VMEM((2 * rows, 128), BF16),
            pltpu.VMEM((2 * rows, 256), F32),
            pltpu.VMEM((2 * rows, 128), F32),
            pltpu.VMEM((rows, 256), F32),
            pltpu.VMEM((rows, 128), F32),
            pltpu.VMEM((tok, 128), F32),
            pltpu.VMEM((tok, 128), F32),
            pltpu.VMEM((4, tok // 4, d), BF16),
            pltpu.VMEM(queries.shape, BF16),
            pltpu.VMEM(keys_raw.shape, BF16),
            pltpu.VMEM((1, 128), F32),
            pltpu.VMEM((1, 128), F32),
            pltpu.VMEM((4, 2, 256, d), BF16),
            pltpu.VMEM((1, d), F32),
            pltpu.VMEM((1, 128), F32),
            pltpu.VMEM((3 * NZ * NX * 2, 32, units), BF16),
            pltpu.VMEM((4, tok, width), BF16),
            pltpu.VMEM((tok, d), F32),
            pltpu.VMEM((4, tok // 4, d), BF16),
            pltpu.VMEM((tok, d), BF16),
            pltpu.VMEM((tok, units), BF16),
            pltpu.VMEM((NZ, 4, tok // 4, 256), BF16),
            pltpu.VMEM((NZ, 2, tok // 8, 256), BF16),
            pltpu.VMEM((NZ, 6, tok // 8, 256), BF16),
            dma((14,)),
            dma((N_SLOTS,)),
            dma,
            dma((3,)),
            dma((3,)),
            dma((3, NZ * NX)),
            dma,
            dma((2 + NZ,)),
            dma,
            dma((3, 6)),
            dma((3, 6)),
            dma,
            dma,
            dma((NZ, 6)),
            dma((NZ, 6)),
        ],
        compiler_params=pltpu.CompilerParams(
            collective_id=0, has_side_effects=True, vmem_limit_bytes=60 * 2**20
        ),
    )(
        residual_in, queries, keys_raw, values_raw, query_gain[None], key_gain[None], out_weight,
        norm_gain[None], gate_weight, up_weight, down_weight.T, freq,
    )


def solution(mesh):
    placed = (
        P(("sp", "tp"), None),
        P("sp", "tp"),
        P("sp", "tp"),
        P("sp", "tp"),
        P(),
        P(),
        P("tp", None),
        P(),
        P("sp", "tp"),
        P("sp", "tp"),
        P("tp", "sp"),
    )
    return jax.shard_map(
        per_device, mesh=mesh, in_specs=placed, out_specs=P(("sp", "tp"), None), check_vma=False
    )
```

time: 117 us -> 104 us (0.89)
  Pallas kernels: 115 us -> 102 us
    pallas_call x1, Pallas kernels: 115 us -> 102 us  [per_device(): pl.pallas_call(layer_kernel, out_shape=jax.ShapeDtypeStruct(residual_in.s...]
where the time goes in v3:
time: 104 us
  Pallas kernels  102 us (98%)
  local copies, waits for them, and re-layouts  1.67 us (2%)
    pallas_call x1, Pallas kernels, per_device(): pl.pallas_call(layer_kernel, out_shape=jax.ShapeDtypeStruct(residual_in.s...  102 us

profile of v3, /device:TPU:1, one launch (start us, length us, event | category | flops | bytes accessed | tf_op | source)
XLA Modules:
  0.0 103.7 jit_solution(4100332555021434536)
XLA Ops:
  0.0 102.0 %shard_map.118 = bf16[64,2048]{1,0:T(8,128)(2,1)} custom-call(bf16[64,2048]{1,0:T(8,128)(2,1)} %res_in.1, bf16[256,512]{1,0:T(8,128)(2,1)} %q_in.1, bf16[256,128]{1,0:T(8,128)(2,1)} %k_in.1, bf16[256,128]{1,0:T(8,128)(2,1)} %v_in.1, f32[1,128]{1,0:T(1,128)} %bitcast.6, f32[1,128]{1,0:T(1,128)} %bitcast.7, bf16[512,2048]{1,0:T(8,128)(2,1)} %wo_in.1, ...), custom_call_target="tpu_custom_call" | custom-call | tf_op jit(solution)/shard_map/pallas_call | solution.py:537
  102.0 1.7 %copy.14 = bf16[64,2048]{1,0:T(8,128)(2,1)} copy(bf16[64,2048]{1,0:T(8,128)(2,1)} %shard_map.118) | data formatting | bytes 524288

commit v4 on v3

--- a/solution.py
+++ b/solution.py
@@ -2,7 +2,6 @@
 
 import jax
 import jax.numpy as jnp
-import numpy as np
 from jax import lax
 from jax.experimental import pallas as pl
 from jax.experimental.pallas import tpu as pltpu
@@ -64,83 +63,90 @@
     return seen
 
 
-W_COLOR = (3, 2, 2)
+W_COLOR = (3, 0, 2)
+GU_PLANES = (0, -1, 1, -2, 2, -3, 3, 4)
+DOWN_PLANES = (0, 1, -1, 2, -2, 3, -3, 4)
+LAG = 6
 SCHEDULE = {
     'start': [
         (3, 0, 0), (4, 0, 0),
     ],
     'chunk0': [
-        (0, 0, 0), (1, 0, 0), (2, 0, 0), (3, 1, 0), (3, -1, 0), (3, 0, 1), (3, 0, -1), (4, 1, 0), (4, -1, 0),
-        (5, 0, 0), (4, 0, 1), (5, 1, 0), (4, 0, -1),
+        (0, 0, 0), (1, 0, 0), (2, 0, 0), (3, 1, 0), (3, -1, 0), (3, 0, -1), (3, 0, 1), (4, 1, 0), (4, 0, 1),
+        (5, 0, 0), (4, -1, 0), (5, 1, 0), (4, 0, -1),
     ],
     'chunk1': [
-        (1, 0, 1), (1, 0, -1), (0, 1, 0), (0, -1, 0), (2, 0, 1), (2, 0, -1), (3, 2, 0), (3, -2, 0), (3, 1, 1),
-        (3, 1, -1), (4, 2, 0), (4, -2, 0), (3, -1, 1), (3, -1, -1),
+        (1, 0, -1), (0, -1, 0), (1, 0, 1), (0, 1, 0), (2, 0, 1), (2, 0, -1), (1, -1, 0), (3, 2, 0),
+        (3, -2, 0), (3, 1, -1), (3, 1, 1), (4, 2, 0), (4, -1, 1), (3, -1, -1), (3, -1, 1),
     ],
     'chunk2': [
-        (4, 1, 1), (4, -1, 1), (3, 0, 2), (4, 1, -1), (4, -1, -1), (4, 0, 2), (1, 0, -2),
+        (3, 0, 2), (4, 0, 2), (4, -1, -1), (4, 1, -1), (4, 1, 1), (4, -2, 0), (2, 0, -2),
     ],
     'chunk3': [
-        (5, 2, 0), (5, 3, 0), (3, 2, 1), (3, 2, -1), (3, -2, 1), (3, 3, 0), (3, -3, 0), (0, -2, 0),
-        (2, 0, -2), (3, -2, -1), (0, 2, 0), (4, 3, 0), (4, -3, 0),
+        (5, 2, 0), (5, 3, 0), (3, 2, -1), (3, 3, 0), (1, 0, 2), (1, -1, -1), (1, -1, 1), (3, -2, -1),
+        (1, 1, 0), (0, -2, 0), (4, 3, 0), (3, -3, 0), (3, 1, -2), (3, 2, 1), (4, 1, 2),
     ],
     'chunk4': [
-        (3, 1, -2), (4, 2, 1), (4, -2, 1), (3, -1, -2), (3, 2, 2), (4, 2, -1), (4, -2, -1), (1, -1, 0),
-        (3, 3, -1),
+        (4, -2, 1), (4, -1, 2), (4, 2, -1), (4, 2, 1), (3, -2, 1), (3, 3, 1), (3, 3, -1), (3, -1, -2),
+        (1, -2, 0),
     ],
     'chunk5': [
-        (3, -2, 2), (4, 1, 2), (4, -1, 2), (3, -3, -1), (3, 3, 1), (3, 4, 0), (3, -3, 1), (0, -3, 0),
-        (1, -1, -1), (1, 1, 0), (4, -3, 1), (0, 3, 0),
+        (4, -2, -1), (3, 4, 0), (4, -3, 0), (3, -3, 1), (0, 2, 0), (1, -1, -2), (1, 1, 1), (1, 1, -1),
+        (0, -3, 0), (3, 2, 2), (3, -3, -1), (4, 4, 0), (4, -3, 1), (3, -2, 2),
     ],
     'chunk6': [
-        (3, 3, -2), (4, 4, 0), (4, -3, -1), (3, 4, 1), (3, -3, -2), (4, 3, 1), (1, -1, 1), (2, 1, 0),
-        (0, 0, 1), (3, 4, -1), (4, 3, -1),
+        (4, 2, 2), (4, 3, -1), (4, -2, 2), (3, 3, -2), (1, 2, 0), (0, 0, -1), (1, -2, -1), (1, -2, 1),
+        (3, 4, 1), (4, 3, 1), (3, 4, -1),
     ],
     'chunk7': [
-        (4, -2, 2), (4, 2, 2), (3, 4, 2), (0, 0, -1), (1, 1, 1), (1, 1, -1), (0, -4, 0), (2, 1, -1),
-        (4, -4, 1), (1, -1, 2), (1, -2, 0), (1, 2, 0), (4, -4, -1), (2, 1, 1), (0, 0, -2), (1, 1, 2),
-        (4, 3, 2), (4, -3, 2), (0, -1, 1), (1, -2, -1), (0, 1, 1), (1, -2, 1), (2, -1, 0), (1, 2, -1),
-        (0, 1, -1), (1, 2, 1), (0, -1, -1), (1, 3, 0), (1, -2, -2), (2, 2, 0), (2, 1, 2), (0, -1, -2),
-        (2, -1, -1), (4, 4, 2), (1, -3, 0), (0, 1, -2), (2, -1, 1),
+        (4, -3, -1), (0, 0, 1), (1, 1, -2), (1, -3, 0), (0, 3, 0), (4, 3, 2), (0, -4, 0), (1, 2, 1),
+        (3, -3, -2), (4, -4, 1), (2, 1, 0), (1, -2, 2), (1, 2, -1), (4, -3, 2), (1, 3, 0), (3, 4, 2),
+        (0, -1, -1), (0, 1, -1), (2, -1, 0), (1, -3, 1), (4, -4, -1), (1, -3, -1), (0, 0, -2), (4, 4, 2),
     ],
     'chunk8': [
-        (0, -2, 1), (1, 2, -2), (0, 2, 1), (1, 3, 1), (1, 3, -1),
+        (0, -2, -1), (0, 1, 1), (1, 2, 2), (1, 3, -1), (2, 1, 1), (2, 1, -1),
     ],
     'att': [
-        (0, 2, -1), (0, -2, -1), (2, 2, 1), (2, 2, -1),
+        (1, 3, 1), (1, 4, 0), (0, -1, 1), (2, -1, -1),
     ],
     'own': [
-        (1, -3, 1), (2, 3, 0), (0, -2, -2), (1, -3, -1), (0, 2, -2), (2, -1, 2), (1, -4, 0), (2, 2, -2),
-        (0, 3, 1), (2, -2, 0), (1, 3, 2),
+        (0, 2, -1), (2, -1, 1), (0, -1, -2), (1, -3, -2), (2, 2, 0), (2, 1, 2), (0, -3, -1), (1, 3, -2),
+        (0, 1, -2), (2, -2, 0),
     ],
     'relay': [
-        (0, -3, 1), (2, 3, -1), (0, 3, -1), (1, -3, 2), (0, -3, -1),
+        (0, -2, 1), (1, 4, -1), (1, 4, 1), (0, 2, 1), (2, -1, 2), (0, -2, -2), (2, 2, -1), (0, 3, -1),
     ],
     'two': [
-        (1, -4, -1), (0, 3, -2), (0, -3, -2), (2, 3, 1), (2, -2, -1), (0, 4, 1), (1, -4, 1),
+        (2, 2, 1), (2, 3, 0), (2, -2, -1), (0, 2, -2), (2, -3, 0), (2, -2, 1),
     ],
     'opp': [
-        (2, -3, 0), (0, 4, -1), (2, -2, 1), (1, -4, -2), (0, -4, -2),
-    ],
-    'ffn0': [
-        (2, 3, 2),
-    ],
-    'ffn1': [
+        (0, -3, 1), (2, 2, -2),
+    ],
+    'k1': [
+        (1, 4, 2), (0, -3, -2), (0, 3, 1),
+    ],
+    'k2': [
+        (2, 3, -1),
+    ],
+    'k4': [
+        (0, 4, -1), (2, 3, 1), (2, -4, 0),
+    ],
+    'k5': [
         (2, -2, -2),
     ],
-    'ffn4': [
-        (2, -4, 0), (2, -3, 1),
-    ],
-    'ffn5': [
-        (2, -3, -1),
-    ],
-    'plane3': [
-        (2, -4, -1), (2, -4, 1),
+    'k6': [
+        (0, 3, -2), (2, -3, 1), (0, -4, -2), (2, -3, -1),
+    ],
+    'k7': [
+        (0, 4, 1), (2, 3, 2), (2, -4, -1),
+    ],
+    'plane1': [
+        (2, -4, 1),
     ],
     'plane4': [
         (2, -3, 2),
     ],
-    'plane6': [
+    'plane5': [
         (2, -4, -2),
     ],
 }
@@ -148,8 +154,6 @@
 SLOT_OF = {b: i for i, b in enumerate(SLOTS)}
 N_SLOTS = len(SLOTS)
 PER = 8
-PLANES = (0, 1, -1, 2, -2, 3, -3, 4)
-LAG = 3
 BLOCK = 128
 
 
@@ -163,12 +167,12 @@
 
 
 def layer_kernel(
-    res_in, q_in, k_in, v_in, qg_in, kg_in, wo_in, ng_in, gate_in, up_in, down_in, freq_in, out_ref,
+    res_in, q_in, k_in, v_in, qg_in, kg_in, wo_in, ng_in, gate_in, up_in, down_in, out_hbm,
     kv, qall, acc, top, far_acc, far_top, cos_ref, sin_ref,
-    res_ref, q_ref, k_ref, qg_ref, kg_ref, wo_ref, ng_ref, freq_ref,
-    wbuf, att, proj, mix, rows_ref, hidden, terms, sums, parts,
-    in_sem, kv_recv, kv_send, swap_recv, swap_send,
-    w_recv, w_send, d2d_recv, d2d_send, ring_recv, ring_send, wo_recv, wo_send, rs_recv, rs_send,
+    res_ref, q_ref, k_ref, qg_ref, kg_ref, wo_ref, ng_ref,
+    wbuf, att, proj, mix, rows_ref, gu_ref, hidden, terms, sums, parts, out_ref,
+    in_sem, out_sem, kv_recv, kv_send, swap_recv, swap_send,
+    w_recv, w_send, d2d_recv, d2d_send, ring_recv, ring_send, wo_recv, wo_send, rs_recv, rs_last, rs_send,
 ):
     me = lax.axis_index("sp")
     y = lax.axis_index("tp")
@@ -192,11 +196,10 @@
     for dev in (y_up, y_down):
         pl.semaphore_signal(barrier, inc=1, device_id={"tp": dev}, device_id_type=MESH)
 
-    pairs = [(freq_in, freq_ref), (k_in, k_ref), (kg_in, kg_ref)]
-    pairs += [(v_in.at[pl.ds(h * 128, 128)], kv.at[h, :, pl.ds(128, 128)]) for h in (0, 1)]
+    pairs = [(k_in, k_ref), (kg_in, kg_ref), (v_in, kv.at[pl.ds(0, 2), :, pl.ds(128, 128)])]
     pairs += [(q_in, q_ref), (qg_in, qg_ref)]
     pairs += [(res_in, res_ref.at[y])]
-    pairs += [(wo_in.at[pl.ds(h * 256, 256)], wo_ref.at[0, h]) for h in (0, 1)]
+    pairs += [(wo_in, wo_ref.at[0])]
     pairs += [(w, wbuf.at[2 * (NZ * NX * m + z * NX + x) + core]) for m, w in enumerate((gate_in, up_in, down_in))]
     pairs += [(ng_in, ng_ref)]
     loads = [pltpu.make_async_copy(a, b, in_sem.at[i]) for i, (a, b) in enumerate(pairs)]
@@ -210,11 +213,11 @@
     lane = lax.broadcasted_iota(jnp.int32, (tok, 128), 1)
     token = lax.broadcasted_iota(jnp.int32, (tok, 128), 0) + me * tok
     place = jnp.where(lane < 64, token // GRID_W, token % GRID_W).astype(F32)
-    for load in loads[:5]:
-        load.wait()
-    angle = place * freq_ref[...]
+    angle = place * jnp.exp2((lane % 32).astype(F32) * (-math.log2(THETA) / 32))
     cos_ref[...] = jnp.cos(angle)
     sin_ref[...] = jnp.sin(angle)
+    for load in loads[:3]:
+        load.wait()
     k_rot = rope(k_ref[...].astype(F32), kg_ref[...], cos_ref[...], sin_ref[...], lane)
     for h in (0, 1):
         kv[h, :, 0:128] = k_rot[h * 128 : (h + 1) * 128]
@@ -238,7 +241,7 @@
     def gather_y(n, ref, own, below, above, slot_up, slot_down, far_up, far_down, piece):
         def hop(i, src, dst, k, dev):
             return pltpu.make_async_remote_copy(
-                ref.at[src, *piece(k)], ref.at[dst, *piece(k)], ring_send.at[n, i], ring_recv.at[n, i],
+                ref.at[src, *piece(k)], ref.at[dst, *piece(k)], ring_send.at[n], ring_recv.at[n, i],
                 device_id={"tp": dev}, device_id_type=MESH,
             )
 
@@ -279,11 +282,11 @@
 
     send_on(0)
     send_on(1)
-    for load in loads[7:10]:
+    for load in loads[5:7]:
         load.wait()
     begin(res_ring)
     begin(wo_ring)
-    for load in loads[5:7]:
+    for load in loads[3:5]:
         load.wait()
     for h in range(heads):
         q_rot = rope(
@@ -302,7 +305,7 @@
     swap_q.start()
     acc[...] = jnp.zeros_like(acc)
     top[...] = jnp.full_like(top, -1e30)
-    for load in loads[10:]:
+    for load in loads[7:]:
         load.wait()
 
     def weight_block(m, dz, dx):
@@ -319,7 +322,7 @@
                 device_id={"sp": at[link]}, device_id_type=MESH,
             ).start()
         pltpu.make_async_remote_copy(
-            block, block, d2d_send, d2d_recv.at[m + (dz % NZ if m == 2 else 0)], device_id={"sp": partner}, device_id_type=MESH
+            block, block, d2d_send, d2d_recv.at[m, dz % NZ], device_id={"sp": partner}, device_id_type=MESH
         ).start()
 
     def events(point):
@@ -374,6 +377,9 @@
     swap_top.start()
     attend(last * PER, range(rows // BLOCK, 2 * rows // BLOCK))
     events(f"chunk{last + 1}")
+    for k in (0, 1):
+        wo_ring[2 + k].wait_recv()
+        wo_to_partner(3, k)
     swap_acc.wait_recv()
     swap_top.wait_recv()
     for h in range(heads):
@@ -399,9 +405,6 @@
     att_ring[1][1].wait_recv()
     att_ring[3].start()
     events("relay")
-    for k, (slot, c) in enumerate(((3, wo_ring[2]), (3, wo_ring[3]))):
-        c.wait_recv()
-        wo_to_partner(slot, k)
     shared = wo_ref.at[pl.ds(1, 3), 1 - core]
     from_other = pltpu.make_async_remote_copy(
         shared, shared, wo_send, wo_recv, device_id={"sp": partner}, device_id_type=MESH
@@ -427,30 +430,27 @@
         rows_ref[r] = normed.astype(BF16)
     events("opp")
 
-    def from_partner(i, blocks):
-        whole = wbuf.at[pl.ds(0, blocks)]
-        return pltpu.make_async_remote_copy(
-            whole, whole, d2d_send, d2d_recv.at[i], device_id={"sp": partner}, device_id_type=MESH
-        )
-
-    from_partner(0, NZ * NX).wait_recv()
-    from_partner(1, NZ * NX).wait_recv()
-    events("ffn0")
+    def plane_of(m, dz):
+        four = wbuf.at[pl.ds(0, NX)]
+        pltpu.make_async_remote_copy(
+            four, four, d2d_send, d2d_recv.at[m, dz % NZ], device_id={"sp": partner}, device_id_type=MESH
+        ).wait_recv()
+        return wbuf[pl.ds(2 * (NZ * NX * m + NX * zs[dz]), 2 * NX)].reshape(64 * NX, units)
+
     units = hidden.shape[1]
-    for n in range(units // 128):
-        cols = slice(n * 128, (n + 1) * 128)
-        both = jnp.concatenate(
-            [wbuf[64 * m : 64 * (m + 1), :, cols].reshape(NZ * NX * 64, 128) for m in (0, 1)], axis=1
-        )
-        gu = jnp.dot(rows_ref[...], both, preferred_element_type=F32)
-        gate, up = gu[:, 0:128], gu[:, 128:256]
-        hidden[:, cols] = (gate / (1.0 + jnp.exp(-gate)) * up).astype(BF16)
-        events(f"ffn{n + 1}")
+    for n, dz in enumerate(GU_PLANES):
+        lhs = rows_ref[:, pl.ds(pl.multiple_of(256 * zs[dz], 256), 256)]
+        for m in (0, 1):
+            part = jnp.dot(lhs, plane_of(m, dz), preferred_element_type=F32)
+            gu_ref[m] = part if n == 0 else gu_ref[m] + part
+        events(f"k{n + 1}")
+    gate = gu_ref[0]
+    hidden[...] = (gate / (1.0 + jnp.exp(-gate)) * gu_ref[1]).astype(BF16)
 
     def plane_copies(i):
         def hop(n, src, dev):
             return pltpu.make_async_remote_copy(
-                src, parts.at[i, n], rs_send.at[i, n], rs_recv.at[i, n],
+                src, parts.at[i, n], rs_send, rs_recv.at[i, n] if n < 2 else rs_last,
                 device_id={"tp": dev}, device_id_type=MESH,
             )
 
@@ -474,10 +474,8 @@
         sums[i, 1] = (parts[i, 1].astype(F32) + terms[i, y_down, 32:64].astype(F32)).astype(BF16)
         copies[i][5].start()
 
-    for i, dz in enumerate(PLANES):
-        from_partner(2 + dz % NZ, NX).wait_recv()
-        rhs = wbuf[pl.ds(2 * NZ * NX * 2 + 8 * zs[dz], 8)].reshape(256, units)
-        piece = lax.dot_general(hidden[...], rhs, (((1,), (1,)), ((), ())), preferred_element_type=F32)
+    for i, dz in enumerate(DOWN_PLANES):
+        piece = lax.dot_general(hidden[...], plane_of(2, dz), (((1,), (1,)), ((), ())), preferred_element_type=F32)
         terms[i] = piece.astype(BF16).reshape(4, 64, 256)
         for c in copies[i][:4]:
             c.start()
@@ -486,15 +484,18 @@
             add_and_pass(i - LAG)
     for i in range(NZ - LAG, NZ):
         add_and_pass(i)
-    for i, dz in enumerate(PLANES):
-        for c in copies[i][2:]:
-            c.wait_recv()
+    last_pieces = parts.at[:, pl.ds(2, 4)]
+    pltpu.make_async_remote_copy(
+        last_pieces, last_pieces, rs_send, rs_last, device_id={"tp": y_up}, device_id_type=MESH
+    ).wait_recv()
+    for i, dz in enumerate(DOWN_PLANES):
         cols = pl.ds(pl.multiple_of(256 * zs[dz], 256), 256)
         for h, (a, b) in enumerate(((3, 4), (2, 5))):
             r = slice(32 * h, 32 * (h + 1))
             fed = terms[i, y, r].astype(F32) + parts[i, a].astype(F32) + parts[i, b].astype(F32)
             out_ref[r, cols] = (mix[y, r, cols].astype(F32) + 0.5 * fed).astype(BF16)
-
+    out = pltpu.make_async_copy(out_ref, out_hbm, out_sem)
+    out.start()
     moved = kv.at[pl.ds(0, N_SLOTS - 2)]
     pltpu.make_async_remote_copy(
         moved, moved, kv_send, kv_recv.at[0], device_id={"sp": partner}, device_id_type=MESH
@@ -502,16 +503,18 @@
     for blocks, sem in ((3 * (NZ * NX - 1), w_send), (3 * NZ * NX, d2d_send)):
         moved = wbuf.at[pl.ds(0, blocks)]
         pltpu.make_async_remote_copy(
-            moved, moved, sem, d2d_recv.at[0], device_id={"sp": partner}, device_id_type=MESH
+            moved, moved, sem, d2d_recv.at[0, 0], device_id={"sp": partner}, device_id_type=MESH
         ).wait_send()
-    for ups, downs, a, b in (res_ring, wo_ring, att_ring):
-        for c in (*ups, *downs, a, b):
-            c.wait_send()
+    for n, sent in enumerate((res_ref.at[pl.ds(0, 3)], wo_ref.at[pl.ds(0, 3), 0], att.at[pl.ds(0, 3)])):
+        pltpu.make_async_remote_copy(
+            sent, sent, ring_send.at[n], ring_recv.at[n, 0], device_id={"tp": y_up}, device_id_type=MESH
+        ).wait_send()
     for c in (swap_q, swap_acc, swap_top, from_other):
         c.wait_send()
-    for plane in copies:
-        for c in plane:
-            c.wait_send()
+    pltpu.make_async_remote_copy(
+        parts, parts, rs_send, rs_last, device_id={"tp": y_up}, device_id_type=MESH
+    ).wait_send()
+    out.wait()
 
 
 def per_device(
@@ -531,14 +534,12 @@
     rows = tok * width // 128
     d = residual_in.shape[1]
     units = gate_weight.shape[1]
-    freq = (THETA ** (-np.arange(0, 64, 2, dtype=np.float64) / 64)).astype(np.float32)
-    freq = jnp.asarray(np.tile(freq, 4)[None])
     dma = pltpu.SemaphoreType.DMA
     return pl.pallas_call(
         layer_kernel,
         out_shape=jax.ShapeDtypeStruct(residual_in.shape, BF16),
-        in_specs=[pl.BlockSpec(memory_space=pl.ANY)] * 12,
-        out_specs=pl.BlockSpec(memory_space=pltpu.VMEM),
+        in_specs=[pl.BlockSpec(memory_space=pl.ANY)] * 11,
+        out_specs=pl.BlockSpec(memory_space=pl.ANY),
         scratch_shapes=[
             pltpu.VMEM((N_SLOTS, 128, 256), BF16),
             pltpu.VMEM((2 * rows, 128), BF16),
@@ -555,38 +556,42 @@
             pltpu.VMEM((1, 128), F32),
             pltpu.VMEM((4, 2, 256, d), BF16),
             pltpu.VMEM((1, d), F32),
-            pltpu.VMEM((1, 128), F32),
             pltpu.VMEM((3 * NZ * NX * 2, 32, units), BF16),
             pltpu.VMEM((4, tok, width), BF16),
             pltpu.VMEM((tok, d), F32),
             pltpu.VMEM((4, tok // 4, d), BF16),
             pltpu.VMEM((tok, d), BF16),
+            pltpu.VMEM((2, tok, units), F32),
             pltpu.VMEM((tok, units), BF16),
             pltpu.VMEM((NZ, 4, tok // 4, 256), BF16),
             pltpu.VMEM((NZ, 2, tok // 8, 256), BF16),
             pltpu.VMEM((NZ, 6, tok // 8, 256), BF16),
-            dma((14,)),
+            pltpu.VMEM((tok // 4, d), BF16),
+            dma((11,)),
+            dma,
             dma((N_SLOTS,)),
             dma,
             dma((3,)),
             dma((3,)),
             dma((3, NZ * NX)),
             dma,
-            dma((2 + NZ,)),
+            dma((3, NZ)),
             dma,
             dma((3, 6)),
-            dma((3, 6)),
-            dma,
-            dma,
-            dma((NZ, 6)),
-            dma((NZ, 6)),
+            dma((3,)),
+            dma,
+            dma,
+            dma((NZ, 2)),
+            dma,
+            dma,
         ],
         compiler_params=pltpu.CompilerParams(
             collective_id=0, has_side_effects=True, vmem_limit_bytes=60 * 2**20
         ),
     )(
-        residual_in, queries, keys_raw, values_raw, query_gain[None], key_gain[None], out_weight,
-        norm_gain[None], gate_weight, up_weight, down_weight.T, freq,
+        residual_in, queries, keys_raw, values_raw.reshape(2, 128, 128), query_gain[None], key_gain[None],
+        out_weight.reshape(2, 256, d),
+        norm_gain[None], gate_weight, up_weight, down_weight.T,
     )
 
 

time: 104 us -> 97.9 us (0.941)
  Pallas kernels: 102 us -> 96.1 us
    pallas_call x1, Pallas kernels: 102 us -> 96.1 us  [per_device(): pl.pallas_call(layer_kernel, out_shape=jax.ShapeDtypeStruct(residual_in.s...]
where the time goes in v4:
time: 97.9 us; the launch traced here: 97.8 us
  Pallas kernels  96.1 us (98%)
  local copies, waits for them, and re-layouts  1.67 us (2%)
    pallas_call x1, Pallas kernels, per_device(): pl.pallas_call(layer_kernel, out_shape=jax.ShapeDtypeStruct(residual_in.s...  96.1 us

profile of v4, /device:TPU:1, one launch (start us, length us, event | category | flops | bytes accessed | tf_op | source)
XLA Modules:
  0.0 97.8 jit_solution(2842042534989959765)
XLA Ops:
  0.0 96.1 %shard_map.109 = bf16[64,2048]{1,0:T(8,128)(2,1)} custom-call(bf16[64,2048]{1,0:T(8,128)(2,1)} %res_in.1, bf16[256,512]{1,0:T(8,128)(2,1)} %q_in.1, bf16[256,128]{1,0:T(8,128)(2,1)} %k_in.1, bf16[2,128,128]{2,1,0:T(8,128)(2,1)} %bitcast.8, f32[1,128]{1,0:T(1,128)} %bitcast.10, f32[1,128]{1,0:T(1,128)} %bitcast.11, bf16[2,256,2048]{2,1,0:T(8,128)(2,1)} %bitcast.6, ...), custom_call_target="tpu_custom_call" | custom-call | tf_op jit(solution)/shard_map/pallas_call | solution.py:538
  96.1 1.7 %copy.13 = bf16[64,2048]{1,0:T(8,128)(2,1)} copy(bf16[64,2048]{1,0:T(8,128)(2,1)} %shard_map.109) | data formatting | bytes 524288

commit v5 on v4

--- a/solution.py
+++ b/solution.py
@@ -66,87 +66,84 @@
 W_COLOR = (3, 0, 2)
 GU_PLANES = (0, -1, 1, -2, 2, -3, 3, 4)
 DOWN_PLANES = (0, 1, -1, 2, -2, 3, -3, 4)
-LAG = 6
+LAG = 7
 SCHEDULE = {
     'start': [
         (3, 0, 0), (4, 0, 0),
     ],
     'chunk0': [
-        (0, 0, 0), (1, 0, 0), (2, 0, 0), (3, 1, 0), (3, -1, 0), (3, 0, -1), (3, 0, 1), (4, 1, 0), (4, 0, 1),
-        (5, 0, 0), (4, -1, 0), (5, 1, 0), (4, 0, -1),
+        (0, 0, 0), (1, 0, 0), (2, 0, 0), (3, 1, 0), (3, 0, 1), (3, 0, -1), (3, -1, 0), (4, 1, 0), (4, -1, 0),
+        (5, 0, 0), (4, 0, -1), (5, 1, 0), (4, 0, 1),
     ],
     'chunk1': [
-        (1, 0, -1), (0, -1, 0), (1, 0, 1), (0, 1, 0), (2, 0, 1), (2, 0, -1), (1, -1, 0), (3, 2, 0),
-        (3, -2, 0), (3, 1, -1), (3, 1, 1), (4, 2, 0), (4, -1, 1), (3, -1, -1), (3, -1, 1),
+        (1, 0, -1), (0, 1, 0), (1, 0, 1), (0, -1, 0), (2, 0, 1), (2, 0, -1), (3, 2, 0), (3, 1, 1), (3, -2, 0),
+        (3, 1, -1), (4, 2, 0), (3, 0, 2), (3, -1, -1), (4, -2, 0),
     ],
     'chunk2': [
-        (3, 0, 2), (4, 0, 2), (4, -1, -1), (4, 1, -1), (4, 1, 1), (4, -2, 0), (2, 0, -2),
+        (4, 1, -1), (4, -1, -1), (4, 0, 2), (4, -1, 1), (4, 1, 1), (3, -1, 1), (2, 0, -2),
     ],
     'chunk3': [
-        (5, 2, 0), (5, 3, 0), (3, 2, -1), (3, 3, 0), (1, 0, 2), (1, -1, -1), (1, -1, 1), (3, -2, -1),
-        (1, 1, 0), (0, -2, 0), (4, 3, 0), (3, -3, 0), (3, 1, -2), (3, 2, 1), (4, 1, 2),
+        (5, 2, 0), (5, 3, 0), (3, 2, -1), (3, -3, 0), (3, 2, 1), (3, -2, -1), (3, 1, -2), (3, 3, 0),
+        (0, -2, 0), (1, 0, 2), (1, 1, 0), (4, 3, 0), (3, -2, 1), (3, -1, -2), (4, -3, 0),
     ],
     'chunk4': [
-        (4, -2, 1), (4, -1, 2), (4, 2, -1), (4, 2, 1), (3, -2, 1), (3, 3, 1), (3, 3, -1), (3, -1, -2),
-        (1, -2, 0),
+        (3, -3, -1), (4, 1, 2), (3, -3, 1), (4, 2, -1), (4, -2, -1), (4, -1, 2), (1, -1, 0),
     ],
     'chunk5': [
-        (4, -2, -1), (3, 4, 0), (4, -3, 0), (3, -3, 1), (0, 2, 0), (1, -1, -2), (1, 1, 1), (1, 1, -1),
-        (0, -3, 0), (3, 2, 2), (3, -3, -1), (4, 4, 0), (4, -3, 1), (3, -2, 2),
+        (3, 2, 2), (3, 3, 1), (3, 3, -1), (4, 2, 1), (4, -2, 1), (3, 4, 0), (1, 1, -1), (0, -3, 0), (1, 1, 1),
+        (3, -3, -2), (0, 2, 0), (4, -3, -1),
     ],
     'chunk6': [
-        (4, 2, 2), (4, 3, -1), (4, -2, 2), (3, 3, -2), (1, 2, 0), (0, 0, -1), (1, -2, -1), (1, -2, 1),
-        (3, 4, 1), (4, 3, 1), (3, 4, -1),
+        (3, -2, 2), (4, -2, 2), (4, 2, 2), (3, 3, -2), (4, 4, 0), (1, 2, 0), (1, -1, -1), (1, -1, 1),
+        (1, -2, 0), (3, 4, 1), (3, 4, -1), (4, 3, -1),
     ],
     'chunk7': [
-        (4, -3, -1), (0, 0, 1), (1, 1, -2), (1, -3, 0), (0, 3, 0), (4, 3, 2), (0, -4, 0), (1, 2, 1),
-        (3, -3, -2), (4, -4, 1), (2, 1, 0), (1, -2, 2), (1, 2, -1), (4, -3, 2), (1, 3, 0), (3, 4, 2),
-        (0, -1, -1), (0, 1, -1), (2, -1, 0), (1, -3, 1), (4, -4, -1), (1, -3, -1), (0, 0, -2), (4, 4, 2),
+        (4, 3, 1), (4, -3, 1), (0, 0, -1), (0, -4, 0), (1, 1, -2), (1, 2, 1), (0, 3, 0), (2, 1, 0),
+        (1, 2, -1), (4, -4, -1), (4, 3, 2), (1, -2, 1), (4, -3, 2), (1, -1, -2), (0, 0, 1), (3, 4, 2),
+        (2, -1, 0), (1, -2, -1), (1, -3, 0), (1, 2, 2), (0, 1, -1), (4, -4, 1), (0, 0, -2), (2, 1, 1),
+        (0, -1, -1), (2, 1, -1), (1, 3, 0), (4, 4, 2), (2, 2, 0), (1, -2, 2),
     ],
     'chunk8': [
-        (0, -2, -1), (0, 1, 1), (1, 2, 2), (1, 3, -1), (2, 1, 1), (2, 1, -1),
+        (0, -1, 1), (0, 1, 1), (2, -1, -1), (2, -2, 0), (2, -1, 1),
     ],
     'att': [
-        (1, 3, 1), (1, 4, 0), (0, -1, 1), (2, -1, -1),
+        (1, -3, 1), (0, 2, -1), (1, -3, -1), (1, 3, -1), (0, -1, -2),
     ],
     'own': [
-        (0, 2, -1), (2, -1, 1), (0, -1, -2), (1, -3, -2), (2, 2, 0), (2, 1, 2), (0, -3, -1), (1, 3, -2),
-        (0, 1, -2), (2, -2, 0),
+        (0, 1, -2), (2, 1, 2), (0, -2, -1), (2, 2, -1), (1, 4, 0), (1, 3, 1), (0, -2, 1), (2, -2, -1),
+        (2, 2, 1),
     ],
     'relay': [
-        (0, -2, 1), (1, 4, -1), (1, 4, 1), (0, 2, 1), (2, -1, 2), (0, -2, -2), (2, 2, -1), (0, 3, -1),
+        (2, 3, 0), (1, -3, -2), (0, 2, 1), (2, -2, 1), (0, -2, -2), (2, -3, 0),
     ],
     'two': [
-        (2, 2, 1), (2, 3, 0), (2, -2, -1), (0, 2, -2), (2, -3, 0), (2, -2, 1),
+        (1, 3, -2), (0, -3, -1), (0, 3, -1), (2, -1, 2), (2, 2, -2), (0, 2, -2), (1, 4, 1),
     ],
     'opp': [
-        (0, -3, 1), (2, 2, -2),
+        (0, -3, 1), (1, 4, -1),
     ],
     'k1': [
-        (1, 4, 2), (0, -3, -2), (0, 3, 1),
-    ],
-    'k2': [
-        (2, 3, -1),
+        (0, 3, 1), (0, -3, -2), (2, 3, 1),
+    ],
+    'k3': [
+        (2, -2, -2), (0, 4, -1), (2, -3, 1),
     ],
     'k4': [
-        (0, 4, -1), (2, 3, 1), (2, -4, 0),
-    ],
-    'k5': [
-        (2, -2, -2),
+        (2, -4, 0),
     ],
     'k6': [
-        (0, 3, -2), (2, -3, 1), (0, -4, -2), (2, -3, -1),
+        (0, 3, -2), (2, 3, -1), (1, 4, 2), (0, -4, -2),
     ],
     'k7': [
-        (0, 4, 1), (2, 3, 2), (2, -4, -1),
-    ],
-    'plane1': [
+        (2, -3, -1), (0, 4, 1), (2, 3, 2),
+    ],
+    'k8': [
+        (2, -4, -1), (2, -3, 2),
+    ],
+    'plane3': [
         (2, -4, 1),
     ],
-    'plane4': [
-        (2, -3, 2),
-    ],
-    'plane5': [
+    'plane6': [
         (2, -4, -2),
     ],
 }
@@ -353,25 +350,27 @@
             acc[r, 0:128] = acc[r, 0:128] * shrink + o[:, 0:128]
             acc[r, 128:256] = acc[r, 128:256] * shrink + o[:, 128:256]
 
+    last = N_SLOTS // PER - 1
+
     def chunk(c, _):
         for k in range(1, N_SLOTS // PER - 1):
 
             @pl.when(c == k)
             def _():
                 events(f"chunk{k}")
+                if k == last - 1:
+                    wo_ring[0][1].wait_recv()
+                    wo_to_partner(1, 1)
+                    wo_ring[1][0].wait_recv()
+                    wo_to_partner(2, 0)
 
         attend(c * PER, range(2 * rows // BLOCK))
         return 0
 
-    last = N_SLOTS // PER - 1
     events("chunk0")
     swap_q.wait_recv()
     lax.fori_loop(0, last, chunk, 0)
     events(f"chunk{last}")
-    wo_ring[0][1].wait_recv()
-    wo_to_partner(1, 1)
-    wo_ring[1][0].wait_recv()
-    wo_to_partner(2, 0)
     attend(last * PER, range(rows // BLOCK))
     swap_acc.start()
     swap_top.start()

time: 97.9 us -> 97.4 us (level)
  no operation moved by 1% of the time
where the time goes in v5:
time: 97.4 us; the launch traced here: 97.3 us
  Pallas kernels  95.6 us (98%)
  local copies, waits for them, and re-layouts  1.67 us (2%)
    pallas_call x1, Pallas kernels, per_device(): pl.pallas_call(layer_kernel, out_shape=jax.ShapeDtypeStruct(residual_in.s...  95.6 us

profile of v5, /device:TPU:1, one launch (start us, length us, event | category | flops | bytes accessed | tf_op | source)
XLA Modules:
  0.0 97.3 jit_solution(8048399412014791007)
XLA Ops:
  0.0 95.6 %shard_map.109 = bf16[64,2048]{1,0:T(8,128)(2,1)} custom-call(bf16[64,2048]{1,0:T(8,128)(2,1)} %res_in.1, bf16[256,512]{1,0:T(8,128)(2,1)} %q_in.1, bf16[256,128]{1,0:T(8,128)(2,1)} %k_in.1, bf16[2,128,128]{2,1,0:T(8,128)(2,1)} %bitcast.8, f32[1,128]{1,0:T(1,128)} %bitcast.10, f32[1,128]{1,0:T(1,128)} %bitcast.11, bf16[2,256,2048]{2,1,0:T(8,128)(2,1)} %bitcast.6, ...), custom_call_target="tpu_custom_call" | custom-call | tf_op jit(solution)/shard_map/pallas_call | solution.py:537
  95.6 1.7 %copy.13 = bf16[64,2048]{1,0:T(8,128)(2,1)} copy(bf16[64,2048]{1,0:T(8,128)(2,1)} %shard_map.109) | data formatting | bytes 524288
